TPU v7x, 32 devices: a whole 2x2x4 slice. The times are simulated.
32 devices in a mesh: gr: 2 (over x), fs: 4 (over z), tp: 4 (over y, core).
Axes of the slice: x: 2, y: 2, z: 4, core: 2. Of those that a mesh axis runs over, the one named last changes fastest.
Arguments:
- tokens: bfloat16 [4096, 2048], P(('gr', 'fs', 'tp')), may hold values from -6 to 6
- norm_gain: float32 [2048], P('fs'), may hold values from 0.1 to 1.9
- gate_master: float32 [16, 2048, 256], P(None, 'fs', ('gr', 'tp')), may hold values from -0.125 to 0.125
- up_master: float32 [16, 2048, 256], P(None, 'fs', ('gr', 'tp')), may hold values from -0.125 to 0.125
- down_master: float32 [16, 256, 2048], P(None, 'fs', ('gr', 'tp')), may hold values from -0.375 to 0.375
- route_group: int32 [4096], P(('gr', 'fs', 'tp')), may hold values from 0 to 3
- route_expert: int32 [4096, 2], P(('gr', 'fs', 'tp')), may hold values from 0 to 3, all different within a row
- route_weight: float32 [4096, 2], P(('gr', 'fs', 'tp')), may hold values from 0.1 to 1
Outputs:
- gate_new: bfloat16 [16, 2048, 256], P(('fs', 'tp'))
- up_new: bfloat16 [16, 2048, 256], P(('fs', 'tp'))
- down_new: bfloat16 [16, 256, 2048], P(('fs', 'tp'))
- mixed: bfloat16 [4096, 2048], P(('gr', 'fs', 'tp'))
Inputs may be any that keep to these rules, and one draw needn't show every extreme that they name: `route_expert`: the 2 entries of a row are different.
All inputs are finite; a program needn't handle non-finite values.
Results may differ from a plain program's by a relative error of at most 0.0086.
Values may be sent and summed in bfloat16 or wider, within the bound.
A program may use at most 64 MiB of HBM per device.

v0:
```python
import jax
import jax.numpy as jnp
from jax import lax
from jax.sharding import PartitionSpec as P

E_GROUPS = 4
TOP = 2


def body(
    tokens, norm_gain, gate_master, up_master, down_master, route_group, route_expert, route_weight
):
    n_fs = lax.axis_size("fs")
    n_tp = lax.axis_size("tp")
    n_gr = lax.axis_size("gr")
    experts = n_fs * n_tp
    per_group = experts // E_GROUPS
    gate_cast = (gate_master * norm_gain[None, :, None]).astype(jnp.bfloat16)
    up_cast = (up_master * norm_gain[None, :, None]).astype(jnp.bfloat16)
    down_cast = down_master.astype(jnp.bfloat16)

    def to_grid(tile):
        return tile.reshape((n_fs, n_tp, 1, tile.shape[1], tile.shape[2]))

    grids = (
        to_grid(jnp.swapaxes(gate_cast, 1, 2)),
        to_grid(jnp.swapaxes(up_cast, 1, 2)),
        to_grid(down_cast),
    )
    grids = (
        lax.all_to_all(
            lax.all_to_all(grids[0], "fs", split_axis=0, concat_axis=4, tiled=True),
            "tp",
            split_axis=1,
            concat_axis=3,
            tiled=True,
        ),
        lax.all_to_all(
            lax.all_to_all(grids[1], "fs", split_axis=0, concat_axis=4, tiled=True),
            "tp",
            split_axis=1,
            concat_axis=3,
            tiled=True,
        ),
        lax.all_to_all(
            lax.all_to_all(grids[2], "fs", split_axis=0, concat_axis=4, tiled=True),
            "tp",
            split_axis=1,
            concat_axis=3,
            tiled=True,
        ),
    )
    grids = (
        lax.all_gather(grids[0], "gr", axis=2, tiled=True),
        lax.all_gather(grids[1], "gr", axis=2, tiled=True),
        lax.all_gather(grids[2], "gr", axis=2, tiled=True),
    )

    def rows_to_matrix(grid):
        hidden_units = grid.shape[2] * grid.shape[3]
        return jnp.swapaxes(grid.reshape(hidden_units, grid.shape[4]), 0, 1)[None]

    gate_new = rows_to_matrix(grids[0])
    up_new = rows_to_matrix(grids[1])
    grid = grids[2]
    f_local = grid.shape[3] // n_tp
    d_local = grid.shape[4] // n_fs
    parts = grid.reshape(n_gr, n_tp, f_local, n_fs, d_local)
    parts = jnp.transpose(parts, (3, 2, 0, 1, 4))
    down_new = parts.reshape(1, n_fs * f_local, n_gr * n_tp * d_local)
    width = tokens.shape[1]
    count = tokens.shape[0]
    floats = tokens.astype(jnp.float32)
    normed = (floats * lax.rsqrt(jnp.mean(floats * floats, axis=-1, keepdims=True) + 1e-06)).astype(
        jnp.bfloat16
    )
    capacity = 3 * count * TOP // (2 * experts)
    flat_ids = (route_group[:, None] * per_group + route_expert).reshape(-1)
    columns = lax.broadcasted_iota(jnp.int32, (flat_ids.shape[0], experts), 1)
    onehot = (flat_ids[:, None] == columns).astype(jnp.int32)
    rank = jnp.sum((jnp.cumsum(onehot, axis=0) - 1) * onehot, axis=1)
    dump = experts * capacity
    slot = jnp.where(rank < capacity, flat_ids * capacity + rank, dump)
    rows = jnp.repeat(normed, TOP, axis=0)
    outgoing = (
        jnp.zeros((dump + 1, width), jnp.bfloat16)
        .at[slot]
        .set(rows)[:-1]
        .reshape(experts, capacity, width)
    )
    block = lax.all_to_all(outgoing, ("fs", "tp"), split_axis=0, concat_axis=0, tiled=True)
    flat_rows = block.reshape(-1, width)
    gate = jnp.dot(flat_rows, gate_new[0], preferred_element_type=jnp.float32)
    upper = jnp.dot(flat_rows, up_new[0], preferred_element_type=jnp.float32)
    hidden = (jax.nn.silu(gate) * upper).astype(jnp.bfloat16)
    result = jnp.dot(hidden, down_new[0], preferred_element_type=jnp.float32).astype(jnp.bfloat16)
    outcome = result.reshape(block.shape)
    returned = lax.all_to_all(outcome, ("fs", "tp"), split_axis=0, concat_axis=0, tiled=True)
    table = jnp.concatenate(
        [returned.reshape(-1, width), jnp.zeros((1, width), jnp.bfloat16)], axis=0
    )
    picked = table[slot].reshape(count, TOP, width).astype(jnp.float32)
    mixed = jnp.sum(picked * route_weight[:, :, None], axis=1).astype(jnp.bfloat16)
    return (gate_new, up_new, down_new, mixed)


def solution(mesh):
    placed = (
        P(("gr", "fs", "tp"), None),
        P("fs"),
        P(None, "fs", ("gr", "tp")),
        P(None, "fs", ("gr", "tp")),
        P(None, "fs", ("gr", "tp")),
        P(("gr", "fs", "tp")),
        P(("gr", "fs", "tp"), None),
        P(("gr", "fs", "tp"), None),
    )
    return jax.shard_map(
        body,
        mesh=mesh,
        in_specs=placed,
        out_specs=(
            P(("fs", "tp"), None, None),
            P(("fs", "tp"), None, None),
            P(("fs", "tp"), None, None),
            P(("gr", "fs", "tp"), None),
        ),
        check_vma=False,
    )
```

profile of v0, /device:TPU:0, one launch (start us, length us, event | category | flops | bytes accessed | tf_op | source)
XLA Modules:
  0.0 236.5 jit_solution(1093380789958716760)
XLA Ops:
  7.2 2.6 %multiply_convert_fusion = (bf16[16,512,32]{1,2,0:T(8,128)(2,1)}, bf16[16,512,32]{1,2,0:T(8,128)(2,1)S(1)}) fusion(f32[16,512,32]{1,2,0:T(8,128)} %param.11, f32[512]{0:T(512)} %param.9, f32[16,512,32]{1,2,0:T(8,128)} %param.10), kind=kLoop, calls=%fused_computation.10 | loop fusion | flops 1048576 | bytes 3147776 | tf_op jit(solution)/shard_map/convert_element_type | solution.py:19
  9.8 20.8 %all_to_all.100 = bf16[4,4,1,32,512]{4,3,1,2,0:T(8,128)(2,1)S(1)} all-to-all(bf16[4,4,1,32,512]{4,3,1,2,0:T(8,128)(2,1)S(1)} %bitcast.88), channel_id=1, replica_groups=mesh['gr'=2,'fs'=4,'tp'=4] {'fs'}, dimensions={0} | all-to-all | bytes 1048576 | tf_op jit(solution)/shard_map/all_to_all | solution.py:32
  30.6 3.6 %all-to-all-start.2 = ((bf16[4,4,1,32,512]{4,3,1,2,0:T(8,128)(2,1)}), bf16[4,4,1,32,512]{4,3,1,2,0:T(8,128)(2,1)S(1)}, u32[]{:S(2)}, u32[]{:S(2)}) async-start(bf16[4,4,1,32,512]{4,3,1,2,0:T(8,128)(2,1)} %bitcast.11), calls=%async_computation.2 | async-start | bytes 1048576 | tf_op jit(solution)/shard_map/all_to_all | solution.py:39
  34.2 0.9 convert_element_type.37
  35.0 12.8 %all-to-all-done.2 = bf16[4,4,1,32,512]{4,3,1,2,0:T(8,128)(2,1)S(1)} async-done(((bf16[4,4,1,32,512]{4,3,1,2,0:T(8,128)(2,1)}), bf16[4,4,1,32,512]{4,3,1,2,0:T(8,128)(2,1)S(1)}, u32[]{:S(2)}, u32[]{:S(2)}) %all-to-all-start.2) | async-done | bytes 524320 | tf_op jit(solution)/shard_map/all_to_all | solution.py:39
  47.8 3.6 %all-to-all-start.4 = ((bf16[4,4,1,64,256]{4,3,1,2,0:T(8,128)(2,1)}), bf16[4,4,1,64,256]{4,3,1,2,0:T(8,128)(2,1)S(1)}, u32[]{:S(2)}, u32[]{:S(2)}) async-start(bf16[4,4,1,64,256]{4,3,1,2,0:T(8,128)(2,1)} %bitcast.20), calls=%async_computation.4 | async-start | bytes 1048576 | tf_op jit(solution)/shard_map/all_to_all | solution.py:46
  51.7 0.9 copy.53
  52.6 12.9 %all-to-all-done.4 = bf16[4,4,1,64,256]{4,3,1,2,0:T(8,128)(2,1)S(1)} async-done(((bf16[4,4,1,64,256]{4,3,1,2,0:T(8,128)(2,1)}), bf16[4,4,1,64,256]{4,3,1,2,0:T(8,128)(2,1)S(1)}, u32[]{:S(2)}, u32[]{:S(2)}) %all-to-all-start.4) | async-done | bytes 524320 | tf_op jit(solution)/shard_map/all_to_all | solution.py:46
  65.5 3.5 %all-to-all-start.1 = ((bf16[1,4,1,32,2048]{4,3,2,0,1:T(8,128)(2,1)}), bf16[1,4,1,32,2048]{4,3,2,0,1:T(8,128)(2,1)S(1)}, u32[]{:S(2)}, u32[]{:S(2)}) async-start(bf16[1,4,1,32,2048]{4,3,2,0,1:T(8,128)(2,1)} %bitcast.4), calls=%async_computation.1 | async-start | bytes 1048576 | tf_op jit(solution)/shard_map/all_to_all | solution.py:31
  68.9 0.6 reduce-window.6
  69.5 0.2 fusion.1
  69.7 0.9 copy.54
  70.6 7.1 %all-to-all-done.1 = bf16[1,4,1,32,2048]{4,3,2,0,1:T(8,128)(2,1)S(1)} async-done(((bf16[1,4,1,32,2048]{4,3,2,0,1:T(8,128)(2,1)}), bf16[1,4,1,32,2048]{4,3,2,0,1:T(8,128)(2,1)S(1)}, u32[]{:S(2)}, u32[]{:S(2)}) %all-to-all-start.1) | async-done | bytes 524320 | tf_op jit(solution)/shard_map/all_to_all | solution.py:31
  77.7 3.5 %all-to-all-start.3 = ((bf16[1,4,1,32,2048]{4,3,2,0,1:T(8,128)(2,1)}), bf16[1,4,1,32,2048]{4,3,2,0,1:T(8,128)(2,1)S(1)}, u32[]{:S(2)}, u32[]{:S(2)}) async-start(bf16[1,4,1,32,2048]{4,3,2,0,1:T(8,128)(2,1)} %bitcast.87), calls=%async_computation.3 | async-start | bytes 1048576 | tf_op jit(solution)/shard_map/all_to_all | solution.py:38
  81.2 0.2 fusion.2
  81.4 0.9 copy.55
  82.2 7.8 %all-to-all-done.3 = bf16[1,4,1,32,2048]{4,3,2,0,1:T(8,128)(2,1)S(1)} async-done(((bf16[1,4,1,32,2048]{4,3,2,0,1:T(8,128)(2,1)}), bf16[1,4,1,32,2048]{4,3,2,0,1:T(8,128)(2,1)S(1)}, u32[]{:S(2)}, u32[]{:S(2)}) %all-to-all-start.3) | async-done | bytes 524320 | tf_op jit(solution)/shard_map/all_to_all | solution.py:38
  90.0 4.1 %all-to-all-start.5 = ((bf16[1,4,1,64,1024]{4,3,2,0,1:T(8,128)(2,1)}), bf16[1,4,1,64,1024]{4,3,2,0,1:T(8,128)(2,1)}, u32[]{:S(2)}, u32[]{:S(2)}) async-start(bf16[1,4,1,64,1024]{4,3,2,0,1:T(8,128)(2,1)} %bitcast.23), calls=%async_computation.5 | async-start | bytes 1048576 | tf_op jit(solution)/shard_map/all_to_all | solution.py:45
  94.1 0.2 slice_reduce_fusion
  94.3 0.1 eq.18
  94.6 0.1 mul.70
  94.8 0.6 broadcast_in_dim.28
  95.4 0.4 reshape.146
  95.9 2.6 %scatter_custom_fusion = bf16[385,2048]{1,0:T(8,128)(2,1)S(1)} fusion(s32[256]{0:T(256)S(1)} %bitcast.94, bf16[256,2048]{1,0:T(8,128)(2,1)S(1)} %reshape.146, bf16[]{:T(256)} %constant.11.clone.1), kind=kCustom, calls=%fused_computation.12 | custom fusion | bytes 1576962 | tf_op jit(solution)/shard_map/scatter | solution.py:88
  98.6 1.3 slice.15
  99.8 3.2 %all-to-all-done.5 = bf16[1,4,1,64,1024]{4,3,2,0,1:T(8,128)(2,1)} async-done(((bf16[1,4,1,64,1024]{4,3,2,0,1:T(8,128)(2,1)}), bf16[1,4,1,64,1024]{4,3,2,0,1:T(8,128)(2,1)}, u32[]{:S(2)}, u32[]{:S(2)}) %all-to-all-start.5) | async-done | bytes 524320 | tf_op jit(solution)/shard_map/all_to_all | solution.py:45
  103.0 3.7 %all-to-all-start.6 = ((bf16[16,24,2048]{2,1,0:T(8,128)(2,1)}), bf16[16,24,2048]{2,1,0:T(8,128)(2,1)S(1)}, u32[]{:S(2)}, u32[]{:S(2)}) async-start(bf16[16,24,2048]{2,1,0:T(8,128)(2,1)} %bitcast.30), calls=%async_computation.6 | async-start | bytes 3145728 | tf_op jit(solution)/shard_map/all_to_all | solution.py:91
  106.8 0.7 all-gather.8.cloned.1.call-update
  107.5 0.7 all-gather.4.cloned.1.call-update
  108.3 0.7 all-gather.6.cloned.1.call-update
  108.9 22.7 %all-gather.8.cloned.1.call-done = bf16[1,1,2,256,1024]{4,3,1,0,2:T(8,128)(2,1)} async-done(((bf16[1,1,1,256,1024]{4,3,1,0,2:T(8,128)(2,1)}), bf16[1,1,2,256,1024]{4,3,1,0,2:T(8,128)(2,1)}) %all-gather.8.cloned.1.call-update) | async-done | bytes 1048592 | tf_op jit(solution)/shard_map/all_gather | solution.py:56
  131.7 2.6 %reshape.125 = bf16[2,4,64,4,256]{4,3,2,1,0:T(4,128)(2,1)} reshape(bf16[1,1,2,256,1024]{4,3,1,0,2:T(8,128)(2,1)} %all-gather.8.cloned.1.call-done) | data formatting | bytes 2097152 | tf_op jit(solution)/shard_map/reshape | solution.py:68
  134.3 2.0 copy.46
  136.3 1.6 squeeze_reshape.3
  137.9 17.2 %all-gather.4.cloned.1.call-done = bf16[1,1,2,128,2048]{4,3,1,0,2:T(8,128)(2,1)} async-done(((bf16[1,1,1,128,2048]{4,3,1,0,2:T(8,128)(2,1)}), bf16[1,1,2,128,2048]{4,3,1,0,2:T(8,128)(2,1)}) %all-gather.4.cloned.1.call-update) | async-done | bytes 1048592 | tf_op jit(solution)/shard_map/all_gather | solution.py:54
  155.1 1.8 fusion.15
  156.9 21.6 %all-gather.6.cloned.1.call-done = bf16[1,1,2,128,2048]{4,3,1,0,2:T(8,128)(2,1)} async-done(((bf16[1,1,1,128,2048]{4,3,1,0,2:T(8,128)(2,1)}), bf16[1,1,2,128,2048]{4,3,1,0,2:T(8,128)(2,1)}) %all-gather.6.cloned.1.call-update) | async-done | bytes 1048592 | tf_op jit(solution)/shard_map/all_gather | solution.py:55
  178.5 4.5 %convolution_convert_fusion = bf16[384,2048]{1,0:T(8,128)(2,1)} fusion(bf16[256,2048]{1,0:T(8,128)(2,1)} %squeeze_reshape.3, bf16[384,2048]{1,0:T(8,128)(2,1)S(1)} %bitcast.77, bf16[256,2048]{1,0:T(8,128)(2,1)} %bitcast.90, f32[384,256]{1,0:T(8,128)S(1)} %fusion.15), kind=kOutput, calls=%fused_computation.2 | convolution fusion | flops 806682624 | bytes 5636096 | tf_op jit(solution)/shard_map/dot_general | solution.py:96
  183.1 5.8 %all-to-all-start.7 = ((bf16[16,24,2048]{2,1,0:T(8,128)(2,1)}), bf16[16,24,2048]{2,1,0:T(8,128)(2,1)S(1)}, u32[]{:S(2)}, u32[]{:S(2)}) async-start(bf16[16,24,2048]{2,1,0:T(8,128)(2,1)} %bitcast.89), calls=%async_computation.7 | async-start | bytes 3145728 | tf_op jit(solution)/shard_map/all_to_all | solution.py:98
  189.0 2.3 copy.42
  191.2 2.3 copy.38
  193.5 1.6 reshape.126
  195.1 25.6 %all-to-all-done.7 = bf16[16,24,2048]{2,1,0:T(8,128)(2,1)S(1)} async-done(((bf16[16,24,2048]{2,1,0:T(8,128)(2,1)}), bf16[16,24,2048]{2,1,0:T(8,128)(2,1)S(1)}, u32[]{:S(2)}, u32[]{:S(2)}) %all-to-all-start.7) | async-done | bytes 1572896 | tf_op jit(solution)/shard_map/all_to_all | solution.py:98
  220.7 1.2 copy-done
  221.8 1.5 concatenate.3
  223.4 1.4 gather_fusion
  224.7 1.3 reshape.133
  226.1 3.9 %multiply_reduce_fusion = bf16[128,2048]{1,0:T(8,128)(2,1)} fusion(f32[128,2,2048]{2,1,0:T(2,128)S(1)} %reshape.133, f32[128,2]{1,0:T(8,128)S(1)} %copy.52), kind=kLoop, calls=%fused_computation.3 | loop fusion | flops 786432 | bytes 2622464 | tf_op jit(solution)/shard_map/reduce_sum | solution.py:103
  (32 shorter events, 0.8 us)
Async XLA Ops:
  9.8 24.4 %copy-start.4 = (f32[16,64,256]{2,1,0:T(8,128)S(1)}, f32[16,64,256]{2,1,0:T(8,128)}, u32[]{:S(2)}) copy-start(f32[16,64,256]{2,1,0:T(8,128)} %param.12) | copy-start | bytes 3145732
  30.6 20.9 %copy-start.7 = (s32[128]{0:T(128)S(1)}, s32[128]{0:T(128)}, u32[]{:S(2)}) copy-start(s32[128]{0:T(128)} %param.13) | copy-start | bytes 1540
  30.6 20.9 %copy-start.6 = (s32[128,2]{0,1:T(2,128)S(1)}, s32[128,2]{0,1:T(2,128)}, u32[]{:S(2)}) copy-start(s32[128,2]{0,1:T(2,128)} %param.14) | copy-start | bytes 3076
  30.6 17.3 %all-to-all-start.2 = ((bf16[4,4,1,32,512]{4,3,1,2,0:T(8,128)(2,1)}), bf16[4,4,1,32,512]{4,3,1,2,0:T(8,128)(2,1)S(1)}, u32[]{:S(2)}, u32[]{:S(2)}) async-start(bf16[4,4,1,32,512]{4,3,1,2,0:T(8,128)(2,1)} %bitcast.11), calls=%async_computation.2 | async-start | bytes 1048576 | tf_op jit(solution)/shard_map/all_to_all | solution.py:39
  47.8 21.7 %copy-start.1 = (bf16[128,2048]{1,0:T(8,128)(2,1)S(1)}, bf16[128,2048]{1,0:T(8,128)(2,1)}, u32[]{:S(2)}) copy-start(bf16[128,2048]{1,0:T(8,128)(2,1)} %param.8) | copy-start | bytes 1572868
  47.8 17.6 %all-to-all-start.4 = ((bf16[4,4,1,64,256]{4,3,1,2,0:T(8,128)(2,1)}), bf16[4,4,1,64,256]{4,3,1,2,0:T(8,128)(2,1)S(1)}, u32[]{:S(2)}, u32[]{:S(2)}) async-start(bf16[4,4,1,64,256]{4,3,1,2,0:T(8,128)(2,1)} %bitcast.20), calls=%async_computation.4 | async-start | bytes 1048576 | tf_op jit(solution)/shard_map/all_to_all | solution.py:46
  65.5 12.3 %all-to-all-start.1 = ((bf16[1,4,1,32,2048]{4,3,2,0,1:T(8,128)(2,1)}), bf16[1,4,1,32,2048]{4,3,2,0,1:T(8,128)(2,1)S(1)}, u32[]{:S(2)}, u32[]{:S(2)}) async-start(bf16[1,4,1,32,2048]{4,3,2,0,1:T(8,128)(2,1)} %bitcast.4), calls=%async_computation.1 | async-start | bytes 1048576 | tf_op jit(solution)/shard_map/all_to_all | solution.py:31
  77.7 12.3 %copy-start.2 = (bf16[1,4,1,32,2048]{4,3,2,0,1:T(8,128)(2,1)}, bf16[1,4,1,32,2048]{4,3,2,0,1:T(8,128)(2,1)S(1)}, u32[]{:S(2)}) copy-start(bf16[1,4,1,32,2048]{4,3,2,0,1:T(8,128)(2,1)S(1)} %all-to-all-done.1) | copy-start | bytes 1572868
  77.7 12.3 %all-to-all-start.3 = ((bf16[1,4,1,32,2048]{4,3,2,0,1:T(8,128)(2,1)}), bf16[1,4,1,32,2048]{4,3,2,0,1:T(8,128)(2,1)S(1)}, u32[]{:S(2)}, u32[]{:S(2)}) async-start(bf16[1,4,1,32,2048]{4,3,2,0,1:T(8,128)(2,1)} %bitcast.87), calls=%async_computation.3 | async-start | bytes 1048576 | tf_op jit(solution)/shard_map/all_to_all | solution.py:38
  90.0 5.9 %copy-start.3 = (bf16[1,4,1,32,2048]{4,3,2,0,1:T(8,128)(2,1)}, bf16[1,4,1,32,2048]{4,3,2,0,1:T(8,128)(2,1)S(1)}, u32[]{:S(2)}) copy-start(bf16[1,4,1,32,2048]{4,3,2,0,1:T(8,128)(2,1)S(1)} %all-to-all-done.3) | copy-start | bytes 1572868
  90.0 13.0 %all-to-all-start.5 = ((bf16[1,4,1,64,1024]{4,3,2,0,1:T(8,128)(2,1)}), bf16[1,4,1,64,1024]{4,3,2,0,1:T(8,128)(2,1)}, u32[]{:S(2)}, u32[]{:S(2)}) async-start(bf16[1,4,1,64,1024]{4,3,2,0,1:T(8,128)(2,1)} %bitcast.23), calls=%async_computation.5 | async-start | bytes 1048576 | tf_op jit(solution)/shard_map/all_to_all | solution.py:45
  103.0 52.1 %all-to-all-start.6 = ((bf16[16,24,2048]{2,1,0:T(8,128)(2,1)}), bf16[16,24,2048]{2,1,0:T(8,128)(2,1)S(1)}, u32[]{:S(2)}, u32[]{:S(2)}) async-start(bf16[16,24,2048]{2,1,0:T(8,128)(2,1)} %bitcast.30), calls=%async_computation.6 | async-start | bytes 3145728 | tf_op jit(solution)/shard_map/all_to_all | solution.py:91
  106.7 24.9 %all-gather.8.cloned.1.call-start = ((), (), s32[]{:S(2)}) async-start(), calls=%async_computation.10 | async-start | bytes 1572864 | tf_op jit(solution)/shard_map/all_gather | solution.py:56
  107.5 47.6 %all-gather.4.cloned.1.call-start = ((), (), s32[]{:S(2)}) async-start(), calls=%async_computation.8 | async-start | bytes 1572864 | tf_op jit(solution)/shard_map/all_gather | solution.py:54
  108.2 70.3 %all-gather.6.cloned.1.call-start = ((), (), s32[]{:S(2)}) async-start(), calls=%async_computation.9 | async-start | bytes 1572864 | tf_op jit(solution)/shard_map/all_gather | solution.py:55
  183.1 5.8 %copy-start.5 = (f32[128,2]{0,1:T(2,128)S(1)}, f32[128,2]{0,1:T(2,128)}, u32[]{:S(2)}) copy-start(f32[128,2]{0,1:T(2,128)} %param.15) | copy-start | bytes 3076
  183.1 37.6 %all-to-all-start.7 = ((bf16[16,24,2048]{2,1,0:T(8,128)(2,1)}), bf16[16,24,2048]{2,1,0:T(8,128)(2,1)S(1)}, u32[]{:S(2)}, u32[]{:S(2)}) async-start(bf16[16,24,2048]{2,1,0:T(8,128)(2,1)} %bitcast.89), calls=%async_computation.7 | async-start | bytes 3145728 | tf_op jit(solution)/shard_map/all_to_all | solution.py:98
  220.7 1.2 copy-start
Sparse Core Ops, SparseCore 0:
  109.1 22.5 all-gather.7
  133.8 21.2 all-gather.3
  157.2 21.2 all-gather.5
where the time goes:
time: 241 us; the launch traced here: 237 us
  waiting for transfers between devices  133 us (55%)
  starting transfers between devices  27.9 us (12%)
  local copies, waits for them, and re-layouts  26.2 us (11%)
  blocking collectives  20.8 us (9%)
  between operations  14 us (6%)
  other arithmetic  8.51 us (4%)
  matrix products  6.36 us (3%)
    all_to_all x1, waiting for transfers between devices, body(): lax.all_to_all(outcome, ('fs', 'tp'), split_axis=0, concat_axis=0, tiled=...  25.6 us
    all_gather x1, waiting for transfers between devices, body(): lax.all_gather(grids[2], 'gr', axis=2, tiled=True)  22.7 us
    all_gather x1, waiting for transfers between devices, body(): lax.all_gather(grids[1], 'gr', axis=2, tiled=True)  21.6 us
    all_to_all x1, blocking collectives, body(): lax.all_to_all(grids[0], 'fs', split_axis=0, concat_axis=4, tiled=True)  20.8 us
    all_gather x1, waiting for transfers between devices, body(): lax.all_gather(grids[0], 'gr', axis=2, tiled=True)  17.2 us
    all_to_all x1, waiting for transfers between devices, body(): lax.all_to_all(grids[2], 'fs', split_axis=0, concat_axis=4, tiled=True)  12.9 us
    all_to_all x1, waiting for transfers between devices, body(): lax.all_to_all(grids[1], 'fs', split_axis=0, concat_axis=4, tiled=True)  12.8 us
    all_to_all x1, waiting for transfers between devices, body(): lax.all_to_all(lax.all_to_all(grids[1], 'fs', split_axis=0, concat_axis=4...  7.76 us
  transfers between devices with their start and end apart: 10, of which 9 were waited for; matrix products, arithmetic and copies ran while one was open for 10% of the time, Pallas kernels for 0%

commit v1 on v0

v1 whole, which is shorter than its diff:
```python
import functools

import jax
import jax.numpy as jnp
from jax import lax
from jax.experimental import pallas as pl
from jax.experimental.pallas import tpu as pltpu
from jax.sharding import PartitionSpec as P

E_GROUPS = 4
TOP = 2
MESH = pl.DeviceIdType.MESH
ANY = pl.BlockSpec(memory_space=pl.ANY)


def place(expert, n_tp):
    return {"fs": expert // n_tp, "tp": lax.rem(expert, n_tp)}


def greet(me, experts, n_tp, my_gr, n_gr):
    barrier = pltpu.get_barrier_semaphore()

    def hello(step, carry):
        pl.semaphore_signal(
            barrier,
            inc=1,
            device_id=place(lax.rem(me + step, experts), n_tp),
            device_id_type=MESH,
        )
        return carry

    lax.fori_loop(1, experts, hello, 0)
    for step in range(1, n_gr):
        pl.semaphore_signal(
            barrier, inc=1, device_id={"gr": lax.rem(my_gr + step, n_gr)}, device_id_type=MESH
        )
    pl.semaphore_wait(barrier, experts - 1 + n_gr - 1)


def send(src, dst, send_sem, recv_sem, where):
    return pltpu.make_async_remote_copy(
        src_ref=src,
        dst_ref=dst,
        send_sem=send_sem,
        recv_sem=recv_sem,
        device_id=where,
        device_id_type=MESH,
    )


def wait_bytes(ref, sem):
    pltpu.make_async_copy(ref, ref, sem).wait()


def weights_kernel(
    n_gr,
    n_fs,
    n_tp,
    gu,
    dn,
    tok,
    gu_out,
    dn_out,
    tok_out,
    gu_recv,
    dn_recv,
    send_sems,
    relay_send,
    relay_recv,
    tok_recv,
    own_sems,
):
    experts = n_fs * n_tp
    my_gr = lax.axis_index("gr")
    me = lax.axis_index("fs") * n_tp + lax.axis_index("tp")
    greet(me, experts, n_tp, my_gr, n_gr)
    own = (
        pltpu.make_async_copy(gu.at[me], gu_out.at[my_gr, me], own_sems.at[0]),
        pltpu.make_async_copy(dn.at[me], dn_out.at[my_gr, me], own_sems.at[1]),
        pltpu.make_async_copy(tok.at[me], tok_out.at[me], tok_recv),
    )
    for copy in own:
        copy.start()

    def start_weights(step, carry):
        to = lax.rem(me + step, experts)
        where = place(to, n_tp)
        send(gu.at[to], gu_out.at[my_gr, me], send_sems.at[0], gu_recv.at[me], where).start()
        send(dn.at[to], dn_out.at[my_gr, me], send_sems.at[1], dn_recv.at[me], where).start()
        return carry

    lax.fori_loop(1, experts, start_weights, 0)

    def start_tokens(step, carry):
        to = lax.rem(me + step, experts)
        send(tok.at[to], tok_out.at[me], send_sems.at[2], tok_recv, place(to, n_tp)).start()
        return carry

    lax.fori_loop(1, experts, start_tokens, 0)

    def relay(gu_from, dn_from, source):
        for step in range(1, n_gr):
            other = lax.rem(my_gr + step, n_gr)
            where = {"gr": other}
            send(
                gu_from,
                gu_out.at[my_gr, source],
                relay_send.at[0, step],
                relay_recv.at[0, step],
                where,
            ).start()
            send(
                dn_from,
                dn_out.at[my_gr, source],
                relay_send.at[1, step],
                relay_recv.at[1, step],
                where,
            ).start()

    relay(gu.at[me], dn.at[me], me)

    def arrive(step, carry):
        source = lax.rem(me + experts - step, experts)
        where = place(source, n_tp)
        landed_gu = gu_out.at[my_gr, source]
        landed_dn = dn_out.at[my_gr, source]
        send(landed_gu, landed_gu, send_sems.at[0], gu_recv.at[source], where).wait_recv()
        send(landed_dn, landed_dn, send_sems.at[1], dn_recv.at[source], where).wait_recv()
        relay(landed_gu, landed_dn, source)
        return carry

    lax.fori_loop(1, experts, arrive, 0)
    own[0].wait()
    own[1].wait()
    rest = pl.ds(0, experts - 1)
    wait_bytes(gu.at[rest], send_sems.at[0])
    wait_bytes(dn.at[rest], send_sems.at[1])
    wait_bytes(tok.at[rest], send_sems.at[2])
    wait_bytes(tok, tok_recv)
    for step in range(1, n_gr):
        wait_bytes(gu, relay_send.at[0, step])
        wait_bytes(dn, relay_send.at[1, step])
        wait_bytes(gu, relay_recv.at[0, step])
        wait_bytes(dn, relay_recv.at[1, step])


def return_kernel(n_gr, n_fs, n_tp, rows, rows_out, send_sem, recv_sem):
    experts = n_fs * n_tp
    me = lax.axis_index("fs") * n_tp + lax.axis_index("tp")
    greet(me, experts, n_tp, 0, 1)
    pltpu.make_async_copy(rows.at[me], rows_out.at[me], recv_sem).start()

    def start(step, carry):
        to = lax.rem(me + step, experts)
        send(rows.at[to], rows_out.at[me], send_sem, recv_sem, place(to, n_tp)).start()
        return carry

    lax.fori_loop(1, experts, start, 0)
    wait_bytes(rows.at[pl.ds(0, experts - 1)], send_sem)
    wait_bytes(rows, recv_sem)


def body(
    tokens, norm_gain, gate_master, up_master, down_master, route_group, route_expert, route_weight
):
    n_fs = lax.axis_size("fs")
    n_tp = lax.axis_size("tp")
    n_gr = lax.axis_size("gr")
    experts = n_fs * n_tp
    per_group = experts // E_GROUPS
    d_local, f_local = gate_master.shape[1:]
    gate_cast = (gate_master * norm_gain[None, :, None]).astype(jnp.bfloat16)
    up_cast = (up_master * norm_gain[None, :, None]).astype(jnp.bfloat16)
    gu = jnp.concatenate([jnp.swapaxes(gate_cast, 1, 2), jnp.swapaxes(up_cast, 1, 2)], axis=1)
    dn = down_master.astype(jnp.bfloat16)

    count, width = tokens.shape
    floats = tokens.astype(jnp.float32)
    normed = (floats * lax.rsqrt(jnp.mean(floats * floats, axis=-1, keepdims=True) + 1e-06)).astype(
        jnp.bfloat16
    )
    capacity = 3 * count * TOP // (2 * experts)
    pairs = count * TOP
    flat_ids = (route_group[:, None] * per_group + route_expert).reshape(-1)
    columns = lax.broadcasted_iota(jnp.int32, (pairs, experts), 1)
    chosen = flat_ids[:, None] == columns
    earlier = lax.broadcasted_iota(jnp.int32, (pairs, pairs), 1) < lax.broadcasted_iota(
        jnp.int32, (pairs, pairs), 0
    )
    before = jnp.dot(
        earlier.astype(jnp.bfloat16),
        chosen.astype(jnp.bfloat16),
        preferred_element_type=jnp.float32,
    )
    rank = jnp.sum(jnp.where(chosen, before, 0.0), axis=1).astype(jnp.int32)
    dump = experts * capacity
    slot = jnp.where(rank < capacity, flat_ids * capacity + rank, dump).reshape(count, TOP)
    slots = lax.broadcasted_iota(jnp.int32, (count, dump), 1)
    picks = [(slot[:, k][:, None] == slots).astype(jnp.bfloat16) for k in range(TOP)]
    outgoing = lax.dot_general(
        sum(picks[1:], picks[0]),
        normed,
        (((0,), (0,)), ((), ())),
        preferred_element_type=jnp.float32,
    ).astype(jnp.bfloat16)
    outgoing = outgoing.reshape(experts, capacity, width)

    def shape(*dims):
        return jax.ShapeDtypeStruct(dims, jnp.bfloat16)

    dma = pltpu.SemaphoreType.DMA
    gu_all, dn_all, block = pl.pallas_call(
        functools.partial(weights_kernel, n_gr, n_fs, n_tp),
        name="handover",
        out_shape=(shape(n_gr, *gu.shape), shape(n_gr, *dn.shape), shape(*outgoing.shape)),
        in_specs=[ANY] * 3,
        out_specs=(ANY,) * 3,
        scratch_shapes=[
            dma((experts,)),
            dma((experts,)),
            dma((3,)),
            dma((2, n_gr)),
            dma((2, n_gr)),
            dma,
            dma((2,)),
        ],
        compiler_params=pltpu.CompilerParams(collective_id=0, has_side_effects=True),
    )(gu, dn, outgoing)

    tiles = gu_all.reshape(n_gr, n_fs, n_tp, 2, f_local, d_local)
    gate_up = jnp.transpose(tiles, (3, 1, 5, 0, 2, 4)).reshape(
        2, 1, n_fs * d_local, n_gr * n_tp * f_local
    )
    gate_new, up_new = gate_up[0], gate_up[1]
    fz, dw = dn.shape[1:]
    down_new = jnp.transpose(dn_all.reshape(n_gr, n_fs, n_tp, fz, dw), (1, 3, 0, 2, 4)).reshape(
        1, n_fs * fz, n_gr * n_tp * dw
    )

    flat_rows = block.reshape(-1, width)
    gate = jnp.dot(flat_rows, gate_new[0], preferred_element_type=jnp.float32)
    upper = jnp.dot(flat_rows, up_new[0], preferred_element_type=jnp.float32)
    hidden = (jax.nn.silu(gate) * upper).astype(jnp.bfloat16)
    result = jnp.dot(hidden, down_new[0], preferred_element_type=jnp.float32).astype(jnp.bfloat16)
    returned = pl.pallas_call(
        functools.partial(return_kernel, n_gr, n_fs, n_tp),
        name="give_back",
        out_shape=shape(*block.shape),
        in_specs=[ANY],
        out_specs=ANY,
        scratch_shapes=[dma, dma],
        compiler_params=pltpu.CompilerParams(collective_id=1, has_side_effects=True),
    )(result.reshape(block.shape))
    table = returned.reshape(dump, width)
    mixed = sum(
        jnp.dot(picks[k], table, preferred_element_type=jnp.float32) * route_weight[:, k][:, None]
        for k in range(TOP)
    ).astype(jnp.bfloat16)
    return (gate_new, up_new, down_new, mixed)


def solution(mesh):
    placed = (
        P(("gr", "fs", "tp"), None),
        P("fs"),
        P(None, "fs", ("gr", "tp")),
        P(None, "fs", ("gr", "tp")),
        P(None, "fs", ("gr", "tp")),
        P(("gr", "fs", "tp")),
        P(("gr", "fs", "tp"), None),
        P(("gr", "fs", "tp"), None),
    )
    return jax.shard_map(
        body,
        mesh=mesh,
        in_specs=placed,
        out_specs=(
            P(("fs", "tp"), None, None),
            P(("fs", "tp"), None, None),
            P(("fs", "tp"), None, None),
            P(("gr", "fs", "tp"), None),
        ),
        check_vma=False,
    )
```

time: 241 us -> 146 us (0.61)
  the two profiles are of different devices: /device:TPU:0 before, /device:TPU:13 now
where the time goes in v1:
time: 146 us
  Pallas kernels  112 us (77%)
  local copies, waits for them, and re-layouts  18.6 us (13%)
  matrix products  11 us (8%)
  other arithmetic  4.26 us (3%)
    pallas_call x1, Pallas kernels, body(): pl.pallas_call(functools.partial(weights_kernel, n_gr, n_fs, n_tp), name=...  73.3 us
    pallas_call x1, Pallas kernels, body(): pl.pallas_call(functools.partial(return_kernel, n_gr, n_fs, n_tp), name='...  38.2 us
    unnamed x23, local copies, waits for them, and re-layouts  7.65 us
    dot_general x1, matrix products, body(): jnp.dot(hidden, down_new[0], preferred_element_type=jnp.float32)  5.02 us
    reshape x1, local copies, waits for them, and re-layouts, body(): tiles = gu_all.reshape(n_gr, n_fs, n_tp, 2, f_local, d_local)  3.36 us
    dot_general x2, matrix products, body(): jnp.dot(picks[k], table, preferred_element_type=jnp.float32)  3.3 us

profile of v1, /device:TPU:13, one launch (start us, length us, event | category | flops | bytes accessed | tf_op | source)
XLA Modules:
  0.0 146.2 jit_solution(594652160610404375)
XLA Ops:
  0.6 0.0 copy-start.1
  0.6 0.8 copy.20
  1.5 0.7 broadcast_multiply_fusion
  2.1 0.1 broadcast_add_fusion
  2.2 0.1 eq.30
  2.4 0.0 copy-start.5
  2.4 0.0 copy-start.6
  2.4 0.0 copy-start.7
  2.4 0.2 fusion.3
  2.6 0.1 convert_element_type.46
  2.8 0.1 add_select_fusion
  2.9 0.2 slice_reduce_fusion.1
  3.0 1.2 fusion.4
  4.3 0.0 copy-done.1
  4.3 1.8 %convolution_convert_fusion.1 = bf16[384,2048]{1,0:T(8,128)(2,1)} fusion(bf16[128,2048]{1,0:T(8,128)(2,1)S(1)} %copy-done.1, f32[128]{0:T(128)S(1)} %add_rsqrt_fusion, s32[128]{0:T(128)S(1)} %get-tuple-element.19, s32[128]{0:T(128)S(1)} %get-tuple-element.18), kind=kOutput, calls=%fused_computation.1 | convolution fusion | flops 203292672 | bytes 2098688 | tf_op jit(solution)/shard_map/dot_general | solution.py:200
  6.1 0.0 copy-done.5
  6.1 0.0 copy-done.6
  6.1 0.0 copy-done.7
  6.1 0.3 fusion.6
  6.4 0.0 copy-start.3
  6.4 1.0 pad_maximum_fusion.gu
  7.5 0.6 copy-done.3
  8.0 0.9 convert_element_type.44.dn
  8.9 73.3 %handover.1 = (bf16[2,16,64,512]{3,2,1,0:T(8,128)(2,1)}, bf16[2,16,64,256]{3,2,1,0:T(8,128)(2,1)}, bf16[16,24,2048]{2,1,0:T(8,128)(2,1)}) custom-call(bf16[16,64,512]{2,1,0:T(8,128)(2,1)} %pad_maximum_fusion.gu, bf16[16,64,256]{2,1,0:T(8,128)(2,1)} %convert_element_type.44.dn, bf16[16,24,2048]{2,1,0:T(8,128)(2,1)} %bitcast.48), custom_call_target="tpu_custom_call" | custom-call | tf_op jit(solution)/shard_map/handover/pallas_call | solution.py:212
  82.2 3.4 %copy.29 = bf16[2,4,4,2,32,512]{5,1,4,2,0,3:T(4,128)(2,1)S(1)} copy(bf16[2,4,4,2,32,512]{5,4,3,2,1,0:T(8,128)(2,1)} %bitcast.50) | data formatting | bytes 4194304 | tf_op jit(solution)/shard_map/reshape | solution.py:230
  85.6 0.8 fusion.27
  86.3 0.0 copy-start.2
  86.4 0.3 copy.25
  86.6 1.1 copy-done.2
  87.8 0.6 fusion.28
  88.4 0.0 copy-start.4
  88.4 1.2 copy.26
  89.6 0.0 copy-done.4
  89.6 0.8 copy.30
  90.4 1.6 %squeeze_reshape.3 = bf16[256,2048]{1,0:T(8,128)(2,1)} reshape(bf16[4,64,2,4,256]{4,3,2,1,0:T(4,128)(2,1)S(1)} %bitcast.43) | data formatting | bytes 2097152 | tf_op jit(solution)/shard_map/squeeze;reshape | solution.py:244
  92.0 5.0 %convolution_convert_fusion = bf16[384,2048]{1,0:T(8,128)(2,1)} fusion(bf16[256,2048]{1,0:T(8,128)(2,1)} %squeeze_reshape.3, bf16[384,2048]{1,0:T(8,128)(2,1)} %bitcast.51, bf16[2048,256]{0,1:T(8,128)(2,1)} %bitcast.55, f32[384,256]{1,0:T(8,128)S(1)} %fusion.28), kind=kOutput, calls=%fused_computation | convolution fusion | flops 806682624 | bytes 5636096 | tf_op jit(solution)/shard_map/dot_general | solution.py:244
  97.1 0.0 copy-start.8
  97.1 38.2 %give_back.1 = bf16[16,24,2048]{2,1,0:T(8,128)(2,1)} custom-call(bf16[16,24,2048]{2,1,0:T(8,128)(2,1)} %bitcast.53), custom_call_target="tpu_custom_call" | custom-call | tf_op jit(solution)/shard_map/give_back/pallas_call | solution.py:245
  135.3 0.0 copy-start
  135.3 0.0 copy-done.8
  135.3 2.0 %convolution_multiply_fusion.1 = f32[128,2048]{1,0:T(8,128)S(1)} fusion(bf16[384,2048]{1,0:T(8,128)(2,1)} %bitcast.41, f32[128]{0:T(128)S(1)} %get-tuple-element.25, s32[128]{0:T(128)S(1)} %get-tuple-element.18), kind=kOutput, calls=%fused_computation.4 | convolution fusion | flops 201637888 | bytes 2622464 | tf_op jit(solution)/shard_map/dot_general | solution.py:256
  137.3 0.0 copy-done
  137.3 1.3 fusion.1
  138.6 1.6 %squeeze.6 = bf16[1,2048,256]{1,2,0:T(8,128)(2,1)} reshape(bf16[1,4,512,2,4,32]{2,1,5,4,3,0:T(4,128)(2,1)S(1)} %get-tuple-element.21) | data formatting | bytes 2097152 | tf_op jit(solution)/shard_map/squeeze | solution.py:234
  140.2 2.3 %copy.23 = bf16[1,2048,256]{2,1,0:T(8,128)(2,1)} copy(bf16[1,2048,256]{1,2,0:T(8,128)(2,1)} %squeeze.6) | data formatting | bytes 2097152
  142.5 0.8 squeeze.7
  143.3 1.3 copy.24
  144.6 1.6 %reshape.55 = bf16[1,256,2048]{2,1,0:T(8,128)(2,1)} reshape(bf16[4,64,2,4,256]{4,3,2,1,0:T(4,128)(2,1)S(1)} %bitcast.44) | data formatting | bytes 2097152 | tf_op jit(solution)/shard_map/reshape | solution.py:236
  (3 shorter events, 0.0 us)
Async XLA Ops:
  0.6 3.7 %copy-start.1 = (bf16[128,2048]{1,0:T(8,128)(2,1)S(1)}, bf16[128,2048]{1,0:T(8,128)(2,1)}, u32[]{:S(2)}) copy-start(bf16[128,2048]{1,0:T(8,128)(2,1)} %param.8) | copy-start | bytes 1572868
  2.4 3.8 %copy-start.5 = (f32[16,512,32]{1,2,0:T(8,128)S(1)}, f32[16,512,32]{1,2,0:T(8,128)}, u32[]{:S(2)}) copy-start(f32[16,512,32]{1,2,0:T(8,128)} %param.10) | copy-start | bytes 3145732
  2.4 3.8 %copy-start.6 = (f32[16,512,32]{1,2,0:T(8,128)S(1)}, f32[16,512,32]{1,2,0:T(8,128)}, u32[]{:S(2)}) copy-start(f32[16,512,32]{1,2,0:T(8,128)} %param.11) | copy-start | bytes 3145732
  2.4 3.7 %copy-start.7 = (f32[512]{0:T(512)S(1)}, f32[512]{0:T(512)}, u32[]{:S(2)}) copy-start(f32[512]{0:T(512)} %param.9) | copy-start | bytes 6148
  6.4 1.6 %copy-start.3 = (f32[16,64,256]{2,1,0:T(8,128)S(1)}, f32[16,64,256]{2,1,0:T(8,128)}, u32[]{:S(2)}) copy-start(f32[16,64,256]{2,1,0:T(8,128)} %param.12) | copy-start | bytes 3145732
  86.3 1.4 copy-start.2
  88.4 1.3 copy-start.4
  97.1 38.2 %copy-start.8 = (f32[128,2]{0,1:T(2,128)S(1)}, f32[128,2]{0,1:T(2,128)}, u32[]{:S(2)}) copy-start(f32[128,2]{0,1:T(2,128)} %param.15) | copy-start | bytes 3076
  135.3 2.0 %copy-start = (bf16[16,24,2048]{2,1,0:T(8,128)(2,1)S(1)}, bf16[16,24,2048]{2,1,0:T(8,128)(2,1)}, u32[]{:S(2)}) copy-start(bf16[16,24,2048]{2,1,0:T(8,128)(2,1)} %give_back.1) | copy-start | bytes 4718596

commit v2 on v1

--- a/solution.py
+++ b/solution.py
@@ -52,66 +52,90 @@
     pltpu.make_async_copy(ref, ref, sem).wait()
 
 
-def weights_kernel(
+def fused_kernel(
     n_gr,
     n_fs,
     n_tp,
     gu,
     dn,
     tok,
-    gu_out,
-    dn_out,
-    tok_out,
+    gu_full,
+    dn_full,
+    returned,
+    gu_land,
+    dn_land,
+    tok_land,
+    result,
+    gu_whole,
+    dn_whole,
     gu_recv,
     dn_recv,
+    tok_recv,
     send_sems,
     relay_send,
     relay_recv,
-    tok_recv,
+    ret_recv,
     own_sems,
+    out_sems,
 ):
     experts = n_fs * n_tp
     my_gr = lax.axis_index("gr")
-    me = lax.axis_index("fs") * n_tp + lax.axis_index("tp")
+    my_fs = lax.axis_index("fs")
+    my_tp = lax.axis_index("tp")
+    me = my_fs * n_tp + my_tp
+    f_two, d_local = gu.shape[1:]
+    f_local = f_two // 2
+    fz, dw = dn.shape[1:]
+    units = n_gr * n_tp * f_local
+
+    def target(step):
+        return lax.rem(my_fs + step // n_tp, n_fs) * n_tp + lax.rem(my_tp + step, n_tp)
+
+    def origin(step):
+        return lax.rem(my_fs + n_fs - step // n_tp, n_fs) * n_tp + lax.rem(
+            my_tp + n_tp - lax.rem(step, n_tp), n_tp
+        )
+
     greet(me, experts, n_tp, my_gr, n_gr)
     own = (
-        pltpu.make_async_copy(gu.at[me], gu_out.at[my_gr, me], own_sems.at[0]),
-        pltpu.make_async_copy(dn.at[me], dn_out.at[my_gr, me], own_sems.at[1]),
-        pltpu.make_async_copy(tok.at[me], tok_out.at[me], tok_recv),
+        pltpu.make_async_copy(gu.at[me], gu_land.at[my_gr, me], own_sems.at[0]),
+        pltpu.make_async_copy(dn.at[me], dn_land.at[my_gr, me], own_sems.at[1]),
+        pltpu.make_async_copy(tok.at[me], tok_land.at[me], tok_recv.at[me]),
     )
     for copy in own:
         copy.start()
 
     def start_weights(step, carry):
-        to = lax.rem(me + step, experts)
+        to = target(step)
         where = place(to, n_tp)
-        send(gu.at[to], gu_out.at[my_gr, me], send_sems.at[0], gu_recv.at[me], where).start()
-        send(dn.at[to], dn_out.at[my_gr, me], send_sems.at[1], dn_recv.at[me], where).start()
+        send(gu.at[to], gu_land.at[my_gr, me], send_sems.at[0], gu_recv.at[me], where).start()
+        send(dn.at[to], dn_land.at[my_gr, me], send_sems.at[1], dn_recv.at[me], where).start()
         return carry
 
     lax.fori_loop(1, experts, start_weights, 0)
 
     def start_tokens(step, carry):
-        to = lax.rem(me + step, experts)
-        send(tok.at[to], tok_out.at[me], send_sems.at[2], tok_recv, place(to, n_tp)).start()
+        to = target(step)
+        send(
+            tok.at[to], tok_land.at[me], send_sems.at[2], tok_recv.at[me], place(to, n_tp)
+        ).start()
         return carry
 
     lax.fori_loop(1, experts, start_tokens, 0)
 
     def relay(gu_from, dn_from, source):
         for step in range(1, n_gr):
-            other = lax.rem(my_gr + step, n_gr)
-            where = {"gr": other}
+            where = {"gr": lax.rem(my_gr + step, n_gr)}
             send(
                 gu_from,
-                gu_out.at[my_gr, source],
+                gu_land.at[my_gr, source],
                 relay_send.at[0, step],
                 relay_recv.at[0, step],
                 where,
             ).start()
             send(
                 dn_from,
-                dn_out.at[my_gr, source],
+                dn_land.at[my_gr, source],
                 relay_send.at[1, step],
                 relay_recv.at[1, step],
                 where,
@@ -120,10 +144,10 @@
     relay(gu.at[me], dn.at[me], me)
 
     def arrive(step, carry):
-        source = lax.rem(me + experts - step, experts)
+        source = origin(step)
         where = place(source, n_tp)
-        landed_gu = gu_out.at[my_gr, source]
-        landed_dn = dn_out.at[my_gr, source]
+        landed_gu = gu_land.at[my_gr, source]
+        landed_dn = dn_land.at[my_gr, source]
         send(landed_gu, landed_gu, send_sems.at[0], gu_recv.at[source], where).wait_recv()
         send(landed_dn, landed_dn, send_sems.at[1], dn_recv.at[source], where).wait_recv()
         relay(landed_gu, landed_dn, source)
@@ -132,32 +156,74 @@
     lax.fori_loop(1, experts, arrive, 0)
     own[0].wait()
     own[1].wait()
+    for step in range(1, n_gr):
+        wait_bytes(gu, relay_recv.at[0, step])
+        wait_bytes(dn, relay_recv.at[1, step])
+
+    def assemble(part, carry):
+        g = part // n_tp
+        t = lax.rem(part, n_tp)
+        rows = pl.multiple_of(part * f_local, f_local)
+        cols = pl.multiple_of(part * dw, dw)
+        for z in range(n_fs):
+            tile = gu_land[g, z * n_tp + t]
+            width = pl.ds(z * d_local, d_local)
+            gu_whole[pl.ds(rows, f_local), width] = tile[:f_local]
+            gu_whole[pl.ds(units + rows, f_local), width] = tile[f_local:]
+            dn_whole[pl.ds(z * fz, fz), pl.ds(cols, dw)] = dn_land[g, z * n_tp + t]
+        return carry
+
+    lax.fori_loop(0, n_gr * n_tp, assemble, 0)
+
+    def give(step):
+        source = origin(step)
+        send(
+            result.at[source], returned.at[me], send_sems.at[3], ret_recv, place(source, n_tp)
+        ).start()
+
+    def work(step, carry):
+        source = origin(step)
+        landed = tok_land.at[source]
+        pltpu.make_async_copy(landed, landed, tok_recv.at[source]).wait()
+        both = lax.dot_general(
+            tok_land[source],
+            gu_whole[...],
+            (((1,), (1,)), ((), ())),
+            preferred_element_type=jnp.float32,
+        )
+        gate, upper = both[:, :units], both[:, units:]
+        hidden = (gate / (1.0 + jnp.exp(-gate)) * upper).astype(jnp.bfloat16)
+        result[source] = jnp.dot(
+            hidden, dn_whole[...], preferred_element_type=jnp.float32
+        ).astype(jnp.bfloat16)
+
+        @pl.when(step > 1)
+        def _():
+            give(step - 1)
+
+        return carry
+
+    lax.fori_loop(0, experts, work, 0)
+    give(experts - 1)
+    kept = pltpu.make_async_copy(result.at[me], returned.at[me], ret_recv)
+    kept.start()
+    outs = (
+        pltpu.make_async_copy(gu_whole, gu_full, out_sems.at[0]),
+        pltpu.make_async_copy(dn_whole, dn_full, out_sems.at[1]),
+    )
+    for copy in outs:
+        copy.start()
     rest = pl.ds(0, experts - 1)
     wait_bytes(gu.at[rest], send_sems.at[0])
     wait_bytes(dn.at[rest], send_sems.at[1])
     wait_bytes(tok.at[rest], send_sems.at[2])
-    wait_bytes(tok, tok_recv)
     for step in range(1, n_gr):
         wait_bytes(gu, relay_send.at[0, step])
         wait_bytes(dn, relay_send.at[1, step])
-        wait_bytes(gu, relay_recv.at[0, step])
-        wait_bytes(dn, relay_recv.at[1, step])
-
-
-def return_kernel(n_gr, n_fs, n_tp, rows, rows_out, send_sem, recv_sem):
-    experts = n_fs * n_tp
-    me = lax.axis_index("fs") * n_tp + lax.axis_index("tp")
-    greet(me, experts, n_tp, 0, 1)
-    pltpu.make_async_copy(rows.at[me], rows_out.at[me], recv_sem).start()
-
-    def start(step, carry):
-        to = lax.rem(me + step, experts)
-        send(rows.at[to], rows_out.at[me], send_sem, recv_sem, place(to, n_tp)).start()
-        return carry
-
-    lax.fori_loop(1, experts, start, 0)
-    wait_bytes(rows.at[pl.ds(0, experts - 1)], send_sem)
-    wait_bytes(rows, recv_sem)
+    for copy in outs:
+        copy.wait()
+    wait_bytes(tok.at[rest], send_sems.at[3])
+    wait_bytes(tok, ret_recv)
 
 
 def body(
@@ -209,48 +275,38 @@
         return jax.ShapeDtypeStruct(dims, jnp.bfloat16)
 
     dma = pltpu.SemaphoreType.DMA
-    gu_all, dn_all, block = pl.pallas_call(
-        functools.partial(weights_kernel, n_gr, n_fs, n_tp),
-        name="handover",
-        out_shape=(shape(n_gr, *gu.shape), shape(n_gr, *dn.shape), shape(*outgoing.shape)),
+    vmem = functools.partial(pltpu.VMEM, dtype=jnp.bfloat16)
+    units = n_gr * n_tp * f_local
+    full = (2 * units, n_fs * d_local)
+    down_full = (n_fs * dn.shape[1], n_gr * n_tp * dn.shape[2])
+    gu_full, dn_full, returned = pl.pallas_call(
+        functools.partial(fused_kernel, n_gr, n_fs, n_tp),
+        name="experts",
+        out_shape=(shape(*full), shape(*down_full), shape(*outgoing.shape)),
         in_specs=[ANY] * 3,
         out_specs=(ANY,) * 3,
         scratch_shapes=[
+            vmem((n_gr, *gu.shape)),
+            vmem((n_gr, *dn.shape)),
+            vmem(outgoing.shape),
+            vmem(outgoing.shape),
+            vmem(full),
+            vmem(down_full),
             dma((experts,)),
             dma((experts,)),
-            dma((3,)),
+            dma((experts,)),
+            dma((4,)),
             dma((2, n_gr)),
             dma((2, n_gr)),
             dma,
             dma((2,)),
+            dma((2,)),
         ],
         compiler_params=pltpu.CompilerParams(collective_id=0, has_side_effects=True),
     )(gu, dn, outgoing)
-
-    tiles = gu_all.reshape(n_gr, n_fs, n_tp, 2, f_local, d_local)
-    gate_up = jnp.transpose(tiles, (3, 1, 5, 0, 2, 4)).reshape(
-        2, 1, n_fs * d_local, n_gr * n_tp * f_local
-    )
-    gate_new, up_new = gate_up[0], gate_up[1]
-    fz, dw = dn.shape[1:]
-    down_new = jnp.transpose(dn_all.reshape(n_gr, n_fs, n_tp, fz, dw), (1, 3, 0, 2, 4)).reshape(
-        1, n_fs * fz, n_gr * n_tp * dw
-    )
-
-    flat_rows = block.reshape(-1, width)
-    gate = jnp.dot(flat_rows, gate_new[0], preferred_element_type=jnp.float32)
-    upper = jnp.dot(flat_rows, up_new[0], preferred_element_type=jnp.float32)
-    hidden = (jax.nn.silu(gate) * upper).astype(jnp.bfloat16)
-    result = jnp.dot(hidden, down_new[0], preferred_element_type=jnp.float32).astype(jnp.bfloat16)
-    returned = pl.pallas_call(
-        functools.partial(return_kernel, n_gr, n_fs, n_tp),
-        name="give_back",
-        out_shape=shape(*block.shape),
-        in_specs=[ANY],
-        out_specs=ANY,
-        scratch_shapes=[dma, dma],
-        compiler_params=pltpu.CompilerParams(collective_id=1, has_side_effects=True),
-    )(result.reshape(block.shape))
+    gate_new = jnp.swapaxes(gu_full[:units], 0, 1)[None]
+    up_new = jnp.swapaxes(gu_full[units:], 0, 1)[None]
+    down_new = dn_full[None]
     table = returned.reshape(dump, width)
     mixed = sum(
         jnp.dot(picks[k], table, preferred_element_type=jnp.float32) * route_weight[:, k][:, None]

time: 146 us -> 135 us (0.925)
  the two profiles are of different devices: /device:TPU:13 before, /device:TPU:0 now
where the time goes in v2:
time: 135 us
  Pallas kernels  118 us (87%)
  local copies, waits for them, and re-layouts  6.09 us (5%)
  matrix products  5.34 us (4%)
  other arithmetic  4.26 us (3%)
    pallas_call x1, Pallas kernels, body(): pl.pallas_call(functools.partial(fused_kernel, n_gr, n_fs, n_tp), name='e...  118 us
    unnamed x22, local copies, waits for them, and re-layouts  5.5 us
    dot_general x2, matrix products, body(): jnp.dot(picks[k], table, preferred_element_type=jnp.float32)  3.29 us

profile of v2, /device:TPU:0, one launch (start us, length us, event | category | flops | bytes accessed | tf_op | source)
XLA Modules:
  0.0 134.8 jit_solution(9990301712546010709)
XLA Ops:
  0.6 0.0 copy-start.2
  0.6 0.8 copy.17
  1.5 0.7 broadcast_multiply_fusion
  2.1 0.1 broadcast_add_fusion
  2.2 0.1 eq.30
  2.4 0.0 copy-start.5
  2.4 0.0 copy-start.6
  2.4 0.0 copy-start.7
  2.4 0.2 fusion.2
  2.6 0.1 convert_element_type.40
  2.8 0.1 add_select_fusion
  2.9 0.2 slice_reduce_fusion.1
  3.0 1.2 fusion.3
  4.3 0.0 copy-done.2
  4.3 1.8 %convolution_convert_fusion = bf16[384,2048]{1,0:T(8,128)(2,1)} fusion(bf16[128,2048]{1,0:T(8,128)(2,1)S(1)} %copy-done.2, f32[128]{0:T(128)S(1)} %add_rsqrt_fusion, s32[128]{0:T(128)S(1)} %get-tuple-element.23, s32[128]{0:T(128)S(1)} %get-tuple-element.22), kind=kOutput, calls=%fused_computation | convolution fusion | flops 203292672 | bytes 2098688 | tf_op jit(solution)/shard_map/dot_general | solution.py:266
  6.1 0.0 copy-done.5
  6.1 0.0 copy-done.6
  6.1 0.0 copy-done.7
  6.1 0.3 fusion.5
  6.4 0.0 copy-start.3
  6.4 1.0 pad_maximum_fusion.gu
  7.5 0.6 copy-done.3
  8.0 0.9 convert_element_type.38.dn
  8.9 0.0 copy-start.8
  8.9 118.3 %experts.1 = (bf16[512,2048]{1,0:T(8,128)(2,1)}, bf16[256,2048]{1,0:T(8,128)(2,1)}, bf16[16,24,2048]{2,1,0:T(8,128)(2,1)}) custom-call(bf16[16,64,512]{2,1,0:T(8,128)(2,1)} %pad_maximum_fusion.gu, bf16[16,64,256]{2,1,0:T(8,128)(2,1)} %convert_element_type.38.dn, bf16[16,24,2048]{2,1,0:T(8,128)(2,1)} %bitcast.23), custom_call_target="tpu_custom_call" | custom-call | tf_op jit(solution)/shard_map/experts/pallas_call | solution.py:282
  127.2 0.0 copy-start
  127.2 0.0 copy-done.8
  127.2 2.0 %convolution_multiply_fusion.1 = f32[128,2048]{1,0:T(8,128)S(1)} fusion(bf16[384,2048]{1,0:T(8,128)(2,1)} %bitcast.21, f32[128]{0:T(128)S(1)} %get-tuple-element.29, s32[128]{0:T(128)S(1)} %get-tuple-element.22), kind=kOutput, calls=%fused_computation.3 | convolution fusion | flops 201637888 | bytes 2622464 | tf_op jit(solution)/shard_map/dot_general | solution.py:312
  129.2 0.0 copy-done
  129.3 0.0 copy-start.1
  129.3 1.3 fusion.1
  130.6 0.5 copy-done.1
  131.0 0.1 slice_bitcast_fusion
  131.2 1.3 copy.18
  132.5 0.0 copy-start.4
  132.5 1.3 copy.19
  133.8 0.0 copy-done.4
  133.8 1.0 copy.21
  (3 shorter events, 0.0 us)
Async XLA Ops:
  0.6 3.7 %copy-start.2 = (bf16[128,2048]{1,0:T(8,128)(2,1)S(1)}, bf16[128,2048]{1,0:T(8,128)(2,1)}, u32[]{:S(2)}) copy-start(bf16[128,2048]{1,0:T(8,128)(2,1)} %param.8) | copy-start | bytes 1572868
  2.4 3.8 %copy-start.5 = (f32[16,512,32]{1,2,0:T(8,128)S(1)}, f32[16,512,32]{1,2,0:T(8,128)}, u32[]{:S(2)}) copy-start(f32[16,512,32]{1,2,0:T(8,128)} %param.10) | copy-start | bytes 3145732
  2.4 3.8 %copy-start.6 = (f32[16,512,32]{1,2,0:T(8,128)S(1)}, f32[16,512,32]{1,2,0:T(8,128)}, u32[]{:S(2)}) copy-start(f32[16,512,32]{1,2,0:T(8,128)} %param.11) | copy-start | bytes 3145732
  2.4 3.7 %copy-start.7 = (f32[512]{0:T(512)S(1)}, f32[512]{0:T(512)}, u32[]{:S(2)}) copy-start(f32[512]{0:T(512)} %param.9) | copy-start | bytes 6148
  6.4 1.6 %copy-start.3 = (f32[16,64,256]{2,1,0:T(8,128)S(1)}, f32[16,64,256]{2,1,0:T(8,128)}, u32[]{:S(2)}) copy-start(f32[16,64,256]{2,1,0:T(8,128)} %param.12) | copy-start | bytes 3145732
  8.9 118.3 %copy-start.8 = (f32[128,2]{0,1:T(2,128)S(1)}, f32[128,2]{0,1:T(2,128)}, u32[]{:S(2)}) copy-start(f32[128,2]{0,1:T(2,128)} %param.15) | copy-start | bytes 3076
  127.2 2.0 %copy-start = (bf16[16,24,2048]{2,1,0:T(8,128)(2,1)S(1)}, bf16[16,24,2048]{2,1,0:T(8,128)(2,1)}, u32[]{:S(2)}) copy-start(bf16[16,24,2048]{2,1,0:T(8,128)(2,1)} %get-tuple-element.9) | copy-start | bytes 4718596
  129.3 1.8 %copy-start.1 = (bf16[512,2048]{1,0:T(8,128)(2,1)S(1)}, bf16[512,2048]{1,0:T(8,128)(2,1)}, u32[]{:S(2)}) copy-start(bf16[512,2048]{1,0:T(8,128)(2,1)} %get-tuple-element.7) | copy-start | bytes 6291460
  132.5 1.3 copy-start.4

commit v3 on v2

--- a/solution.py
+++ b/solution.py
@@ -226,6 +226,283 @@
     wait_bytes(tok, ret_recv)
 
 
+def plane_kernel(
+    n_gr,
+    n_fs,
+    n_tp,
+    gu,
+    dn,
+    rows,
+    facts,
+    gu_full,
+    dn_full,
+    returned,
+    gu_land,
+    dn_land,
+    row_land,
+    fact_land,
+    block_out,
+    block_land,
+    result_out,
+    result_land,
+    mix_out,
+    gu_whole,
+    dn_whole,
+    gu_recv,
+    dn_recv,
+    row_recv,
+    fact_recv,
+    block_recv,
+    result_recv,
+    send_sems,
+    relay_send,
+    relay_recv,
+    ret_recv,
+    own_sems,
+    out_sems,
+):
+    experts = n_fs * n_tp
+    my_gr = lax.axis_index("gr")
+    my_fs = lax.axis_index("fs")
+    my_tp = lax.axis_index("tp")
+    me = my_fs * n_tp + my_tp
+    f_two, d_local = gu.shape[1:]
+    f_local = f_two // 2
+    fz, dw = dn.shape[1:]
+    units = n_gr * n_tp * f_local
+    count = rows.shape[1]
+    capacity = block_land.shape[2]
+
+    def target(step):
+        return lax.rem(my_fs + step // n_tp, n_fs) * n_tp + lax.rem(my_tp + step, n_tp)
+
+    def origin(step):
+        return lax.rem(my_fs + n_fs - step // n_tp, n_fs) * n_tp + lax.rem(
+            my_tp + n_tp - lax.rem(step, n_tp), n_tp
+        )
+
+    greet(me, experts, n_tp, my_gr, n_gr)
+    own = (
+        pltpu.make_async_copy(gu.at[me], gu_land.at[my_gr, me], own_sems.at[0]),
+        pltpu.make_async_copy(dn.at[me], dn_land.at[my_gr, me], own_sems.at[1]),
+        pltpu.make_async_copy(rows.at[my_fs], row_land.at[my_fs], row_recv.at[my_fs]),
+        pltpu.make_async_copy(facts.at[my_fs], fact_land.at[my_fs], fact_recv.at[my_fs]),
+    )
+    for copy in own:
+        copy.start()
+
+    def start_weights(step, carry):
+        to = target(step)
+        where = place(to, n_tp)
+        send(gu.at[to], gu_land.at[my_gr, me], send_sems.at[0], gu_recv.at[me], where).start()
+        send(dn.at[to], dn_land.at[my_gr, me], send_sems.at[1], dn_recv.at[me], where).start()
+        return carry
+
+    lax.fori_loop(1, experts, start_weights, 0)
+
+    def start_rows(step, carry):
+        to = lax.rem(my_fs + step, n_fs)
+        where = {"fs": to}
+        send(facts.at[to], fact_land.at[my_fs], send_sems.at[3], fact_recv.at[my_fs], where).start()
+        send(rows.at[to], row_land.at[my_fs], send_sems.at[2], row_recv.at[my_fs], where).start()
+        return carry
+
+    lax.fori_loop(1, n_fs, start_rows, 0)
+
+    def relay(gu_from, dn_from, source):
+        for step in range(1, n_gr):
+            where = {"gr": lax.rem(my_gr + step, n_gr)}
+            send(
+                gu_from,
+                gu_land.at[my_gr, source],
+                relay_send.at[0, step],
+                relay_recv.at[0, step],
+                where,
+            ).start()
+            send(
+                dn_from,
+                dn_land.at[my_gr, source],
+                relay_send.at[1, step],
+                relay_recv.at[1, step],
+                where,
+            ).start()
+
+    relay(gu.at[me], dn.at[me], me)
+
+    def arrive(step, carry):
+        source = origin(step)
+        where = place(source, n_tp)
+        landed_gu = gu_land.at[my_gr, source]
+        landed_dn = dn_land.at[my_gr, source]
+        send(landed_gu, landed_gu, send_sems.at[0], gu_recv.at[source], where).wait_recv()
+        send(landed_dn, landed_dn, send_sems.at[1], dn_recv.at[source], where).wait_recv()
+        relay(landed_gu, landed_dn, source)
+        return carry
+
+    lax.fori_loop(1, experts, arrive, 0)
+    own[0].wait()
+    own[1].wait()
+    for step in range(1, n_gr):
+        wait_bytes(gu, relay_recv.at[0, step])
+        wait_bytes(dn, relay_recv.at[1, step])
+
+    def assemble(part, carry):
+        g = part // n_tp
+        t = lax.rem(part, n_tp)
+        rows = pl.multiple_of(part * f_local, f_local)
+        cols = pl.multiple_of(part * dw, dw)
+        for z in range(n_fs):
+            tile = gu_land[g, z * n_tp + t]
+            width = pl.ds(z * d_local, d_local)
+            gu_whole[pl.ds(rows, f_local), width] = tile[:f_local]
+            gu_whole[pl.ds(units + rows, f_local), width] = tile[f_local:]
+            dn_whole[pl.ds(z * fz, fz), pl.ds(cols, dw)] = dn_land[g, z * n_tp + t]
+        return carry
+
+    lax.fori_loop(0, n_gr * n_tp, assemble, 0)
+
+    def plane_of(step):
+        return lax.rem(my_fs + n_fs - step, n_fs)
+
+    def wait_for(ref, sem):
+        pltpu.make_async_copy(ref, ref, sem).wait()
+
+    def hand_out(step):
+        plane = plane_of(step)
+        wait_for(fact_land.at[plane], fact_recv.at[plane])
+        wait_for(row_land.at[plane], row_recv.at[plane])
+        fact = fact_land[plane]
+        spots = lax.broadcasted_iota(jnp.int32, (capacity, count), 0).astype(jnp.float32) + 1.0
+        block = row_land[plane]
+        for turn in list(range(1, n_tp)) + [0]:
+            to = lax.rem(my_tp + turn, n_tp)
+            wanted = spots + (to * capacity).astype(jnp.float32)
+            hit = wanted == fact[0:1, :count]
+            for k in range(1, TOP):
+                hit = jnp.logical_or(hit, wanted == fact[k : k + 1, :count])
+            taken = jnp.dot(
+                jnp.where(hit, 1.0, 0.0).astype(jnp.bfloat16),
+                block,
+                preferred_element_type=jnp.float32,
+            ).astype(jnp.bfloat16)
+            if turn:
+                block_out[plane, turn - 1] = taken
+            else:
+                block_land[plane, my_tp] = taken
+        for turn in range(1, n_tp):
+            send(
+                block_out.at[plane, turn - 1],
+                block_land.at[plane, my_tp],
+                send_sems.at[4],
+                block_recv.at[plane, my_tp],
+                {"tp": lax.rem(my_tp + turn, n_tp)},
+            ).start()
+
+    def work(step):
+        plane = plane_of(step)
+
+        def give(turn):
+            send(
+                result_out.at[plane, turn - 1],
+                result_land.at[plane, my_tp],
+                send_sems.at[5],
+                result_recv.at[plane],
+                {"tp": lax.rem(my_tp + n_tp - turn, n_tp)},
+            ).start()
+
+        for turn in list(range(1, n_tp)) + [0]:
+            source = lax.rem(my_tp + n_tp - turn, n_tp)
+            if turn:
+                wait_for(block_land.at[plane, source], block_recv.at[plane, source])
+            both = lax.dot_general(
+                block_land[plane, source],
+                gu_whole[...],
+                (((1,), (1,)), ((), ())),
+                preferred_element_type=jnp.float32,
+            )
+            gate, upper = both[:, :units], both[:, units:]
+            hidden = (gate / (1.0 + jnp.exp(-gate)) * upper).astype(jnp.bfloat16)
+            done = jnp.dot(hidden, dn_whole[...], preferred_element_type=jnp.float32).astype(
+                jnp.bfloat16
+            )
+            if turn:
+                result_out[plane, turn - 1] = done
+            else:
+                result_land[plane, my_tp] = done
+            if turn > 1:
+                give(turn - 1)
+        give(n_tp - 1)
+
+    def mix(step):
+        plane = plane_of(step)
+        wait_for(result_out.at[plane], result_recv.at[plane])
+        fact = jnp.transpose(fact_land[plane])[:count]
+        total = None
+        for k in range(TOP):
+            picked = None
+            for t in range(n_tp):
+                spots = lax.broadcasted_iota(jnp.int32, (count, capacity), 1) + (1 + t * capacity)
+                hit = spots.astype(jnp.float32) == fact[:, k : k + 1]
+                term = jnp.dot(
+                    jnp.where(hit, 1.0, 0.0).astype(jnp.bfloat16),
+                    result_land[plane, t],
+                    preferred_element_type=jnp.float32,
+                )
+                picked = term if picked is None else picked + term
+            part = picked * fact[:, TOP + k : TOP + k + 1]
+            total = part if total is None else total + part
+        mix_out[plane] = total.astype(jnp.bfloat16)
+
+    def send_mix(step):
+        plane = plane_of(step)
+        send(
+            mix_out.at[plane], returned.at[my_fs], send_sems.at[6], ret_recv, {"fs": plane}
+        ).start()
+
+    def pipeline(step, carry):
+        @pl.when(step >= 2)
+        def _():
+            mix(step - 2)
+
+        @pl.when(step < n_fs)
+        def _():
+            hand_out(step)
+
+        @pl.when(step > 2)
+        def _():
+            send_mix(step - 2)
+
+        @pl.when(jnp.logical_and(step >= 1, step <= n_fs))
+        def _():
+            work(step - 1)
+
+        return carry
+
+    lax.fori_loop(0, n_fs + 2, pipeline, 0)
+    pltpu.make_async_copy(mix_out.at[my_fs], returned.at[my_fs], ret_recv).start()
+    outs = (
+        pltpu.make_async_copy(gu_whole, gu_full, out_sems.at[0]),
+        pltpu.make_async_copy(dn_whole, dn_full, out_sems.at[1]),
+    )
+    for copy in outs:
+        copy.start()
+    rest = pl.ds(0, experts - 1)
+    others = pl.ds(0, n_fs - 1)
+    wait_bytes(gu.at[rest], send_sems.at[0])
+    wait_bytes(dn.at[rest], send_sems.at[1])
+    wait_bytes(rows.at[others], send_sems.at[2])
+    wait_bytes(facts.at[others], send_sems.at[3])
+    wait_bytes(block_out, send_sems.at[4])
+    wait_bytes(result_out, send_sems.at[5])
+    for step in range(1, n_gr):
+        wait_bytes(gu, relay_send.at[0, step])
+        wait_bytes(dn, relay_send.at[1, step])
+    for copy in outs:
+        copy.wait()
+    wait_bytes(mix_out.at[others], send_sems.at[6])
+    wait_bytes(mix_out, ret_recv)
+
+
 def body(
     tokens, norm_gain, gate_master, up_master, down_master, route_group, route_expert, route_weight
 ):
@@ -261,16 +538,6 @@
     rank = jnp.sum(jnp.where(chosen, before, 0.0), axis=1).astype(jnp.int32)
     dump = experts * capacity
     slot = jnp.where(rank < capacity, flat_ids * capacity + rank, dump).reshape(count, TOP)
-    slots = lax.broadcasted_iota(jnp.int32, (count, dump), 1)
-    picks = [(slot[:, k][:, None] == slots).astype(jnp.bfloat16) for k in range(TOP)]
-    outgoing = lax.dot_general(
-        sum(picks[1:], picks[0]),
-        normed,
-        (((0,), (0,)), ((), ())),
-        preferred_element_type=jnp.float32,
-    ).astype(jnp.bfloat16)
-    outgoing = outgoing.reshape(experts, capacity, width)
-
     def shape(*dims):
         return jax.ShapeDtypeStruct(dims, jnp.bfloat16)
 
@@ -279,39 +546,117 @@
     units = n_gr * n_tp * f_local
     full = (2 * units, n_fs * d_local)
     down_full = (n_fs * dn.shape[1], n_gr * n_tp * dn.shape[2])
-    gu_full, dn_full, returned = pl.pallas_call(
-        functools.partial(fused_kernel, n_gr, n_fs, n_tp),
-        name="experts",
-        out_shape=(shape(*full), shape(*down_full), shape(*outgoing.shape)),
-        in_specs=[ANY] * 3,
-        out_specs=(ANY,) * 3,
-        scratch_shapes=[
-            vmem((n_gr, *gu.shape)),
-            vmem((n_gr, *dn.shape)),
-            vmem(outgoing.shape),
-            vmem(outgoing.shape),
-            vmem(full),
-            vmem(down_full),
-            dma((experts,)),
-            dma((experts,)),
-            dma((experts,)),
-            dma((4,)),
-            dma((2, n_gr)),
-            dma((2, n_gr)),
-            dma,
-            dma((2,)),
-            dma((2,)),
-        ],
-        compiler_params=pltpu.CompilerParams(collective_id=0, has_side_effects=True),
-    )(gu, dn, outgoing)
+    if per_group == n_tp and TOP == 2:
+        kept = rank.reshape(count, TOP) < capacity
+        held = jnp.any(kept, axis=1)
+        most = min(count, capacity * (n_tp - 1))
+        ahead = (
+            (route_group[:, None] == route_group[None, :])
+            & held[None, :]
+            & (
+                lax.broadcasted_iota(jnp.int32, (count, count), 1)
+                < lax.broadcasted_iota(jnp.int32, (count, count), 0)
+            )
+        )
+        spot = jnp.sum(ahead.astype(jnp.int32), axis=1)
+        row = jnp.where(held, route_group * most + spot, n_fs * most)
+        lies = row[:, None] == lax.broadcasted_iota(jnp.int32, (count, n_fs * most), 1)
+        picks = lies.astype(jnp.bfloat16)
+        outgoing = lax.dot_general(
+            picks, normed, (((0,), (0,)), ((), ())), preferred_element_type=jnp.float32
+        ).astype(jnp.bfloat16)
+        outgoing = outgoing.reshape(n_fs, most, width)
+        inside = jnp.where(kept, route_expert * capacity + rank.reshape(count, TOP) + 1, 0)
+        values = [inside[:, k].astype(jnp.float32) for k in range(TOP)]
+        values += [route_weight[:, k] for k in range(TOP)]
+        facts = jnp.stack(
+            [jnp.sum(jnp.where(lies, v[:, None], 0.0), axis=0).reshape(n_fs, most) for v in values],
+            axis=1,
+        )
+        lanes = -(-most // 128) * 128
+        facts = jnp.pad(facts, ((0, 0), (0, 8 - 2 * TOP), (0, lanes - most)))
+        blocks = (n_fs, n_tp, capacity, width)
+        fewer = (n_fs, n_tp - 1, capacity, width)
+        gu_full, dn_full, returned = pl.pallas_call(
+            functools.partial(plane_kernel, n_gr, n_fs, n_tp),
+            name="planes",
+            out_shape=(shape(*full), shape(*down_full), shape(*outgoing.shape)),
+            in_specs=[ANY] * 4,
+            out_specs=(ANY,) * 3,
+            scratch_shapes=[
+                vmem((n_gr, *gu.shape)),
+                vmem((n_gr, *dn.shape)),
+                vmem(outgoing.shape),
+                pltpu.VMEM(facts.shape, jnp.float32),
+                vmem(fewer),
+                vmem(blocks),
+                vmem(fewer),
+                vmem(blocks),
+                vmem(outgoing.shape),
+                vmem(full),
+                vmem(down_full),
+                dma((experts,)),
+                dma((experts,)),
+                dma((n_fs,)),
+                dma((n_fs,)),
+                dma((n_fs, n_tp)),
+                dma((n_fs,)),
+                dma((7,)),
+                dma((2, n_gr)),
+                dma((2, n_gr)),
+                dma,
+                dma((2,)),
+                dma((2,)),
+            ],
+            compiler_params=pltpu.CompilerParams(collective_id=0, has_side_effects=True),
+        )(gu, dn, outgoing, facts)
+        mixed = jnp.dot(
+            picks, returned.reshape(-1, width), preferred_element_type=jnp.float32
+        ).astype(jnp.bfloat16)
+    else:
+        slots = lax.broadcasted_iota(jnp.int32, (count, dump), 1)
+        picks = [(slot[:, k][:, None] == slots).astype(jnp.bfloat16) for k in range(TOP)]
+        outgoing = lax.dot_general(
+            sum(picks[1:], picks[0]),
+            normed,
+            (((0,), (0,)), ((), ())),
+            preferred_element_type=jnp.float32,
+        ).astype(jnp.bfloat16)
+        outgoing = outgoing.reshape(experts, capacity, width)
+
+        gu_full, dn_full, returned = pl.pallas_call(
+            functools.partial(fused_kernel, n_gr, n_fs, n_tp),
+            name="experts",
+            out_shape=(shape(*full), shape(*down_full), shape(*outgoing.shape)),
+            in_specs=[ANY] * 3,
+            out_specs=(ANY,) * 3,
+            scratch_shapes=[
+                vmem((n_gr, *gu.shape)),
+                vmem((n_gr, *dn.shape)),
+                vmem(outgoing.shape),
+                vmem(outgoing.shape),
+                vmem(full),
+                vmem(down_full),
+                dma((experts,)),
+                dma((experts,)),
+                dma((experts,)),
+                dma((4,)),
+                dma((2, n_gr)),
+                dma((2, n_gr)),
+                dma,
+                dma((2,)),
+                dma((2,)),
+            ],
+            compiler_params=pltpu.CompilerParams(collective_id=0, has_side_effects=True),
+        )(gu, dn, outgoing)
+        table = returned.reshape(dump, width)
+        mixed = sum(
+            jnp.dot(picks[k], table, preferred_element_type=jnp.float32) * route_weight[:, k][:, None]
+            for k in range(TOP)
+        ).astype(jnp.bfloat16)
     gate_new = jnp.swapaxes(gu_full[:units], 0, 1)[None]
     up_new = jnp.swapaxes(gu_full[units:], 0, 1)[None]
     down_new = dn_full[None]
-    table = returned.reshape(dump, width)
-    mixed = sum(
-        jnp.dot(picks[k], table, preferred_element_type=jnp.float32) * route_weight[:, k][:, None]
-        for k in range(TOP)
-    ).astype(jnp.bfloat16)
     return (gate_new, up_new, down_new, mixed)
 
 

time: 135 us -> 142 us (1.052)
  other arithmetic: 4.26 us -> 8.94 us
  Pallas kernels: 118 us -> 122 us
  matrix products: 5.34 us -> 3.07 us
    pallas_call x1, Pallas kernels: 118 us -> 122 us  [body(): pl.pallas_call(functools.partial(plane_kernel, n_gr, n_fs, n_tp), name='p...]
    dot_general x3 -> x2, matrix products: 5.14 us -> 2.87 us  [the longest x1 1.59 us: body(): lax.dot_general(picks, normed, (((0,), (0,)), ((), ())), preferred_elemen...]
    unnamed x22 -> x15, local copies, waits for them, and re-layouts: 5.5 us -> 3.63 us
    broadcast_in_dim x1, local copies, waits for them, and re-layouts: 0.14 us -> 1.68 us  [body(): up_new = jnp.swapaxes(gu_full[units:], 0, 1)[None]]
where the time goes in v3:
time: 142 us
  Pallas kernels  122 us (86%)
  other arithmetic  8.94 us (6%)
  local copies, waits for them, and re-layouts  6.9 us (5%)
  matrix products  3.07 us (2%)
    pallas_call x1, Pallas kernels, body(): pl.pallas_call(functools.partial(plane_kernel, n_gr, n_fs, n_tp), name='p...  122 us
    unnamed x15, local copies, waits for them, and re-layouts  3.63 us

profile of v3, /device:TPU:0, one launch (start us, length us, event | category | flops | bytes accessed | tf_op | source)
XLA Modules:
  0.0 141.6 jit_solution(5407500325202367504)
XLA Ops:
  0.6 0.0 copy-start.4
  0.6 0.0 copy-start.3
  0.7 0.0 copy-start.5
  0.7 1.4 fusion.1
  2.0 0.7 broadcast_multiply_fusion.1
  2.7 0.8 slice_bitcast_fusion.3
  3.5 0.7 broadcast_multiply_fusion
  4.1 0.1 copy.26
  4.3 0.1 copy.24
  4.4 0.1 eq.31
  4.5 0.2 fusion
  4.7 0.1 convert_element_type.48
  4.9 0.1 fusion.12
  5.0 0.2 fusion.10
  5.2 0.9 convert_reduce_fusion
  6.1 0.7 add_select_fusion.1
  6.8 0.3 select_reduce_fusion.3
  7.1 0.1 stack_reshape.12
  7.2 0.1 stack_reshape.15
  7.2 0.1 stack_reshape.14
  7.3 0.1 stack_reshape.13
  7.4 0.6 select_maximum_fusion.facts
  8.0 2.1 %convert_element_type.46.dn = bf16[16,64,256]{2,1,0:T(8,128)(2,1)} convert(f32[16,64,256]{2,1,0:T(8,128)} %param.12) | non-fusion elementwise | flops 262144 | bytes 1572864 | tf_op jit(solution)/shard_map/convert_element_type | solution.py:518
  10.1 0.0 copy-done.4
  10.1 0.0 copy-done.3
  10.1 0.0 copy-done.5
  10.1 0.0 copy-start
  10.1 0.3 fusion.3
  10.4 1.0 pad_maximum_fusion.gu
  11.5 0.0 copy-done
  11.5 1.6 %convolution_convert_fusion = bf16[288,2048]{1,0:T(8,128)(2,1)} fusion(bf16[128,2048]{1,0:T(8,128)(2,1)S(1)} %copy-done, f32[128]{0:T(128)S(1)} %add_rsqrt_fusion, s32[128]{0:T(128)S(1)} %add_select_fusion.1), kind=kOutput, calls=%fused_computation | convolution fusion | flops 152408064 | bytes 1704960 | tf_op jit(solution)/shard_map/dot_general | solution.py:565
  13.1 122.0 %planes.1 = (bf16[512,2048]{1,0:T(8,128)(2,1)}, bf16[256,2048]{1,0:T(8,128)(2,1)}, bf16[4,72,2048]{2,1,0:T(8,128)(2,1)}) custom-call(bf16[16,64,512]{2,1,0:T(8,128)(2,1)} %pad_maximum_fusion.gu, bf16[16,64,256]{2,1,0:T(8,128)(2,1)} %convert_element_type.46.dn, bf16[4,72,2048]{2,1,0:T(8,128)(2,1)} %bitcast.20, f32[4,8,128]{2,1,0:T(8,128)} %select_maximum_fusion.facts), custom_call_target="tpu_custom_call" | custom-call | tf_op jit(solution)/shard_map/planes/pallas_call | solution.py:580
  135.0 1.7 %slice_bitcast_fusion = (bf16[1,2048,256]{1,2,0:T(8,128)(2,1)S(1)}, bf16[1,2048,256]{1,2,0:T(8,128)(2,1)S(1)}) fusion(bf16[512,2048]{1,0:T(8,128)(2,1)} %get-tuple-element.7), kind=kLoop, calls=%fused_computation.9 | loop fusion | bytes 4194304 | tf_op jit(solution)/shard_map/broadcast_in_dim | solution.py:658
  136.7 0.0 copy-start.1
  136.7 1.3 copy.28
  138.0 0.0 copy-done.1
  138.1 0.0 copy-start.2
  138.1 1.3 convolution_convert_fusion.1
  139.3 1.3 copy.27
  140.6 0.0 copy-done.2
  140.7 1.0 copy.30
  (3 shorter events, 0.0 us)
Async XLA Ops:
  0.6 9.5 %copy-start.4 = (f32[16,512,32]{1,2,0:T(8,128)S(1)}, f32[16,512,32]{1,2,0:T(8,128)}, u32[]{:S(2)}) copy-start(f32[16,512,32]{1,2,0:T(8,128)} %param.11) | copy-start | bytes 3145732
  0.6 9.5 %copy-start.3 = (f32[16,512,32]{1,2,0:T(8,128)S(1)}, f32[16,512,32]{1,2,0:T(8,128)}, u32[]{:S(2)}) copy-start(f32[16,512,32]{1,2,0:T(8,128)} %param.10) | copy-start | bytes 3145732
  0.7 9.5 %copy-start.5 = (f32[512]{0:T(512)S(1)}, f32[512]{0:T(512)}, u32[]{:S(2)}) copy-start(f32[512]{0:T(512)} %param.9) | copy-start | bytes 6148
  10.1 1.4 copy-start
  136.7 1.3 copy-start.1
  138.1 2.6 %copy-start.2 = (bf16[256,2048]{1,0:T(8,128)(2,1)S(1)}, bf16[256,2048]{1,0:T(8,128)(2,1)}, u32[]{:S(2)}) copy-start(bf16[256,2048]{1,0:T(8,128)(2,1)} %get-tuple-element.8) | copy-start | bytes 3145732

commit v4 on v3

--- a/solution.py
+++ b/solution.py
@@ -367,88 +367,80 @@
     def wait_for(ref, sem):
         pltpu.make_async_copy(ref, ref, sem).wait()
 
+    def join(blocks):
+        wide = blocks.astype(jnp.float32)
+        return wide.reshape(n_tp * capacity, wide.shape[2]).astype(jnp.bfloat16)
+
+    def split(wide):
+        return wide.reshape(n_tp, capacity, wide.shape[1]).astype(jnp.bfloat16)
+
     def hand_out(step):
         plane = plane_of(step)
         wait_for(fact_land.at[plane], fact_recv.at[plane])
         wait_for(row_land.at[plane], row_recv.at[plane])
         fact = fact_land[plane]
-        spots = lax.broadcasted_iota(jnp.int32, (capacity, count), 0).astype(jnp.float32) + 1.0
-        block = row_land[plane]
-        for turn in list(range(1, n_tp)) + [0]:
+        spots = lax.broadcasted_iota(jnp.int32, (n_tp * capacity, count), 0).astype(jnp.float32)
+        spots = spots + 1.0
+        hit = spots == fact[0:1, :count]
+        for k in range(1, TOP):
+            hit = jnp.logical_or(hit, spots == fact[k : k + 1, :count])
+        taken = jnp.dot(
+            jnp.where(hit, 1.0, 0.0).astype(jnp.bfloat16),
+            row_land[plane],
+            preferred_element_type=jnp.float32,
+        )
+        block_out[plane] = split(taken)
+        block_land[plane, my_tp] = block_out[plane, my_tp]
+        for turn in range(1, n_tp):
             to = lax.rem(my_tp + turn, n_tp)
-            wanted = spots + (to * capacity).astype(jnp.float32)
-            hit = wanted == fact[0:1, :count]
-            for k in range(1, TOP):
-                hit = jnp.logical_or(hit, wanted == fact[k : k + 1, :count])
-            taken = jnp.dot(
-                jnp.where(hit, 1.0, 0.0).astype(jnp.bfloat16),
-                block,
-                preferred_element_type=jnp.float32,
-            ).astype(jnp.bfloat16)
-            if turn:
-                block_out[plane, turn - 1] = taken
-            else:
-                block_land[plane, my_tp] = taken
-        for turn in range(1, n_tp):
             send(
-                block_out.at[plane, turn - 1],
+                block_out.at[plane, to],
                 block_land.at[plane, my_tp],
                 send_sems.at[4],
                 block_recv.at[plane, my_tp],
-                {"tp": lax.rem(my_tp + turn, n_tp)},
+                {"tp": to},
             ).start()
 
     def work(step):
         plane = plane_of(step)
-
-        def give(turn):
+        for turn in range(1, n_tp):
+            source = lax.rem(my_tp + n_tp - turn, n_tp)
+            wait_for(block_land.at[plane, source], block_recv.at[plane, source])
+        both = lax.dot_general(
+            join(block_land[plane]),
+            gu_whole[...],
+            (((1,), (1,)), ((), ())),
+            preferred_element_type=jnp.float32,
+        )
+        gate, upper = both[:, :units], both[:, units:]
+        hidden = (gate / (1.0 + jnp.exp(-gate)) * upper).astype(jnp.bfloat16)
+        done = jnp.dot(hidden, dn_whole[...], preferred_element_type=jnp.float32)
+        result_out[plane] = split(done)
+        result_land[plane, my_tp] = result_out[plane, my_tp]
+        for turn in range(1, n_tp):
+            source = lax.rem(my_tp + n_tp - turn, n_tp)
             send(
-                result_out.at[plane, turn - 1],
+                result_out.at[plane, source],
                 result_land.at[plane, my_tp],
                 send_sems.at[5],
                 result_recv.at[plane],
-                {"tp": lax.rem(my_tp + n_tp - turn, n_tp)},
+                {"tp": source},
             ).start()
 
-        for turn in list(range(1, n_tp)) + [0]:
-            source = lax.rem(my_tp + n_tp - turn, n_tp)
-            if turn:
-                wait_for(block_land.at[plane, source], block_recv.at[plane, source])
-            both = lax.dot_general(
-                block_land[plane, source],
-                gu_whole[...],
-                (((1,), (1,)), ((), ())),
+    def mix(step):
+        plane = plane_of(step)
+        wait_for(result_out.at[plane, pl.ds(0, n_tp - 1)], result_recv.at[plane])
+        fact = jnp.transpose(fact_land[plane])[:count]
+        found = join(result_land[plane])
+        spots = lax.broadcasted_iota(jnp.int32, (count, n_tp * capacity), 1) + 1
+        spots = spots.astype(jnp.float32)
+        total = None
+        for k in range(TOP):
+            picked = jnp.dot(
+                jnp.where(spots == fact[:, k : k + 1], 1.0, 0.0).astype(jnp.bfloat16),
+                found,
                 preferred_element_type=jnp.float32,
             )
-            gate, upper = both[:, :units], both[:, units:]
-            hidden = (gate / (1.0 + jnp.exp(-gate)) * upper).astype(jnp.bfloat16)
-            done = jnp.dot(hidden, dn_whole[...], preferred_element_type=jnp.float32).astype(
-                jnp.bfloat16
-            )
-            if turn:
-                result_out[plane, turn - 1] = done
-            else:
-                result_land[plane, my_tp] = done
-            if turn > 1:
-                give(turn - 1)
-        give(n_tp - 1)
-
-    def mix(step):
-        plane = plane_of(step)
-        wait_for(result_out.at[plane], result_recv.at[plane])
-        fact = jnp.transpose(fact_land[plane])[:count]
-        total = None
-        for k in range(TOP):
-            picked = None
-            for t in range(n_tp):
-                spots = lax.broadcasted_iota(jnp.int32, (count, capacity), 1) + (1 + t * capacity)
-                hit = spots.astype(jnp.float32) == fact[:, k : k + 1]
-                term = jnp.dot(
-                    jnp.where(hit, 1.0, 0.0).astype(jnp.bfloat16),
-                    result_land[plane, t],
-                    preferred_element_type=jnp.float32,
-                )
-                picked = term if picked is None else picked + term
             part = picked * fact[:, TOP + k : TOP + k + 1]
             total = part if total is None else total + part
         mix_out[plane] = total.astype(jnp.bfloat16)
@@ -492,8 +484,9 @@
     wait_bytes(dn.at[rest], send_sems.at[1])
     wait_bytes(rows.at[others], send_sems.at[2])
     wait_bytes(facts.at[others], send_sems.at[3])
-    wait_bytes(block_out, send_sems.at[4])
-    wait_bytes(result_out, send_sems.at[5])
+    sent = block_out.at[:, pl.ds(0, n_tp - 1)]
+    wait_bytes(sent, send_sems.at[4])
+    wait_bytes(sent, send_sems.at[5])
     for step in range(1, n_gr):
         wait_bytes(gu, relay_send.at[0, step])
         wait_bytes(dn, relay_send.at[1, step])
@@ -576,7 +569,6 @@
         lanes = -(-most // 128) * 128
         facts = jnp.pad(facts, ((0, 0), (0, 8 - 2 * TOP), (0, lanes - most)))
         blocks = (n_fs, n_tp, capacity, width)
-        fewer = (n_fs, n_tp - 1, capacity, width)
         gu_full, dn_full, returned = pl.pallas_call(
             functools.partial(plane_kernel, n_gr, n_fs, n_tp),
             name="planes",
@@ -588,9 +580,9 @@
                 vmem((n_gr, *dn.shape)),
                 vmem(outgoing.shape),
                 pltpu.VMEM(facts.shape, jnp.float32),
-                vmem(fewer),
                 vmem(blocks),
-                vmem(fewer),
+                vmem(blocks),
+                vmem(blocks),
                 vmem(blocks),
                 vmem(outgoing.shape),
                 vmem(full),

time: 142 us -> 138 us (0.972)
  Pallas kernels: 122 us -> 118 us
    pallas_call x1, Pallas kernels: 122 us -> 118 us  [body(): pl.pallas_call(functools.partial(plane_kernel, n_gr, n_fs, n_tp), name='p...]
where the time goes in v4:
time: 138 us
  Pallas kernels  118 us (86%)
  other arithmetic  8.94 us (6%)
  local copies, waits for them, and re-layouts  6.9 us (5%)
  matrix products  3.07 us (2%)
    pallas_call x1, Pallas kernels, body(): pl.pallas_call(functools.partial(plane_kernel, n_gr, n_fs, n_tp), name='p...  118 us
    unnamed x15, local copies, waits for them, and re-layouts  3.63 us

profile of v4, /device:TPU:0, one launch (start us, length us, event | category | flops | bytes accessed | tf_op | source)
XLA Modules:
  0.0 137.9 jit_solution(5697128281186648183)
XLA Ops:
  0.6 0.0 copy-start.4
  0.6 0.0 copy-start.3
  0.7 0.0 copy-start.5
  0.7 1.4 fusion.1
  2.0 0.7 broadcast_multiply_fusion.1
  2.7 0.8 slice_bitcast_fusion.3
  3.5 0.7 broadcast_multiply_fusion
  4.1 0.1 copy.26
  4.3 0.1 copy.24
  4.4 0.1 eq.31
  4.5 0.2 fusion
  4.7 0.1 convert_element_type.48
  4.9 0.1 fusion.12
  5.0 0.2 fusion.10
  5.2 0.9 convert_reduce_fusion
  6.1 0.7 add_select_fusion.1
  6.8 0.3 select_reduce_fusion.3
  7.1 0.1 stack_reshape.12
  7.2 0.1 stack_reshape.15
  7.2 0.1 stack_reshape.14
  7.3 0.1 stack_reshape.13
  7.4 0.6 select_maximum_fusion.facts
  8.0 2.1 %convert_element_type.46.dn = bf16[16,64,256]{2,1,0:T(8,128)(2,1)} convert(f32[16,64,256]{2,1,0:T(8,128)} %param.12) | non-fusion elementwise | flops 262144 | bytes 1572864 | tf_op jit(solution)/shard_map/convert_element_type | solution.py:511
  10.1 0.0 copy-done.4
  10.1 0.0 copy-done.3
  10.1 0.0 copy-done.5
  10.1 0.0 copy-start
  10.1 0.3 fusion.3
  10.4 1.0 pad_maximum_fusion.gu
  11.5 0.0 copy-done
  11.5 1.6 %convolution_convert_fusion = bf16[288,2048]{1,0:T(8,128)(2,1)} fusion(bf16[128,2048]{1,0:T(8,128)(2,1)S(1)} %copy-done, f32[128]{0:T(128)S(1)} %add_rsqrt_fusion, s32[128]{0:T(128)S(1)} %add_select_fusion.1), kind=kOutput, calls=%fused_computation | convolution fusion | flops 152408064 | bytes 1704960 | tf_op jit(solution)/shard_map/dot_general | solution.py:558
  13.1 118.2 %planes.1 = (bf16[512,2048]{1,0:T(8,128)(2,1)}, bf16[256,2048]{1,0:T(8,128)(2,1)}, bf16[4,72,2048]{2,1,0:T(8,128)(2,1)}) custom-call(bf16[16,64,512]{2,1,0:T(8,128)(2,1)} %pad_maximum_fusion.gu, bf16[16,64,256]{2,1,0:T(8,128)(2,1)} %convert_element_type.46.dn, bf16[4,72,2048]{2,1,0:T(8,128)(2,1)} %bitcast.20, f32[4,8,128]{2,1,0:T(8,128)} %select_maximum_fusion.facts), custom_call_target="tpu_custom_call" | custom-call | tf_op jit(solution)/shard_map/planes/pallas_call | solution.py:572
  131.3 1.7 %slice_bitcast_fusion = (bf16[1,2048,256]{1,2,0:T(8,128)(2,1)S(1)}, bf16[1,2048,256]{1,2,0:T(8,128)(2,1)S(1)}) fusion(bf16[512,2048]{1,0:T(8,128)(2,1)} %get-tuple-element.7), kind=kLoop, calls=%fused_computation.9 | loop fusion | bytes 4194304 | tf_op jit(solution)/shard_map/broadcast_in_dim | solution.py:650
  133.0 0.0 copy-start.1
  133.0 1.3 copy.28
  134.3 0.0 copy-done.1
  134.3 0.0 copy-start.2
  134.3 1.3 convolution_convert_fusion.1
  135.6 1.3 copy.27
  136.9 0.0 copy-done.2
  136.9 1.0 copy.30
  (3 shorter events, 0.0 us)
Async XLA Ops:
  0.6 9.5 %copy-start.4 = (f32[16,512,32]{1,2,0:T(8,128)S(1)}, f32[16,512,32]{1,2,0:T(8,128)}, u32[]{:S(2)}) copy-start(f32[16,512,32]{1,2,0:T(8,128)} %param.11) | copy-start | bytes 3145732
  0.6 9.5 %copy-start.3 = (f32[16,512,32]{1,2,0:T(8,128)S(1)}, f32[16,512,32]{1,2,0:T(8,128)}, u32[]{:S(2)}) copy-start(f32[16,512,32]{1,2,0:T(8,128)} %param.10) | copy-start | bytes 3145732
  0.7 9.5 %copy-start.5 = (f32[512]{0:T(512)S(1)}, f32[512]{0:T(512)}, u32[]{:S(2)}) copy-start(f32[512]{0:T(512)} %param.9) | copy-start | bytes 6148
  10.1 1.4 copy-start
  133.0 1.3 copy-start.1
  134.3 2.6 %copy-start.2 = (bf16[256,2048]{1,0:T(8,128)(2,1)S(1)}, bf16[256,2048]{1,0:T(8,128)(2,1)}, u32[]{:S(2)}) copy-start(bf16[256,2048]{1,0:T(8,128)(2,1)} %get-tuple-element.8) | copy-start | bytes 3145732
